TPU v7x, 32 devices: a whole 2x2x4 slice. The times are simulated.
32 devices in a mesh: sp: 4 (over z), dp: 8 (over y, x, core).
Axes of the slice: x: 2, y: 2, z: 4, core: 2. Of those that a mesh axis runs over, the one named last changes fastest.
Arguments:
- inputs: bfloat16 [8, 512, 2048], P('dp', 'sp'), may hold values from -0.75 to 0.75
- queries: bfloat16 [8, 512, 1024], P('dp', 'sp'), may hold values from -18 to 18
- keys: bfloat16 [8, 512, 256], P('dp', 'sp'), may hold values from -18 to 18
- values: bfloat16 [8, 512, 256], P('dp', 'sp'), may hold values from -6 to 6
- out_grad: bfloat16 [8, 512, 1024], P('dp', 'sp'), may hold values from -144 to 144
- query_gain: float32 [64], replicated, may hold values from 0.4 to 6.5
- key_gain: float32 [64], replicated, may hold values from 0.4 to 6.5
- key_matrix: bfloat16 [2048, 256], P('dp'), may hold values from -0.125 to 0.125
- value_matrix: bfloat16 [2048, 256], P('dp'), may hold values from -0.125 to 0.125
Outputs:
- input_grad: bfloat16 [8, 512, 2048], P('dp', 'sp')
- query_grad: bfloat16 [8, 512, 1024], P('dp', 'sp')
- key_weight_grad: float32 [2048, 256], P('dp')
- value_weight_grad: float32 [2048, 256], P('dp')
All inputs are finite; a program needn't handle non-finite values.
Results may differ from a plain program's by a relative error of at most 0.024.
The roundings to bfloat16 on the way count: a program that leaves them out, or rounds other values in their place, can miss the bound.
Values may be sent and summed in bfloat16 or wider, within the bound.
A program may use at most 64 MiB of HBM per device.

v0:
```python
import functools

import jax
import jax.numpy as jnp
import numpy as np
from jax import lax
from jax.experimental import pallas as pl
from jax.experimental.pallas import tpu as pltpu
from jax.sharding import PartitionSpec as P

QUERY_HEADS = 16
KEY_VALUE_HEADS = 4
HEAD_CHANNELS = 64
GRID = 64


rope_base = 10000.0
norm_eps = 0.5
score_scale = 0.125


def product(pattern, first_op, second_op):
    return jnp.einsum(pattern, first_op, second_op, preferred_element_type=jnp.float32)


def rotary_tables(token_length):
    position = jnp.arange(token_length, dtype=jnp.int32)
    grid_row = (position // GRID).astype(jnp.float32)
    grid_col = (position % GRID).astype(jnp.float32)
    half_pairs = HEAD_CHANNELS // 4
    inv_freq = rope_base ** (-jnp.arange(half_pairs, dtype=jnp.float32) / half_pairs)
    angles = jnp.concatenate([grid_row[:, None] * inv_freq, grid_col[:, None] * inv_freq], axis=1)
    return (jnp.cos(angles), jnp.sin(angles))


def rotate(vector, cos_tab, sin_tab):
    even_part = vector[..., 0::2]
    odd_part = vector[..., 1::2]
    turned = jnp.stack(
        [even_part * cos_tab - odd_part * sin_tab, even_part * sin_tab + odd_part * cos_tab],
        axis=-1,
    )
    return turned.reshape(vector.shape)


def rotate_back(cotangent, cos_tab, sin_tab):
    even_part = cotangent[..., 0::2]
    odd_part = cotangent[..., 1::2]
    turned = jnp.stack(
        [even_part * cos_tab + odd_part * sin_tab, odd_part * cos_tab - even_part * sin_tab],
        axis=-1,
    )
    return turned.reshape(cotangent.shape)


def inverse_rms(vector):
    return lax.rsqrt(jnp.mean(vector * vector, axis=-1, keepdims=True) + norm_eps)


def norm_back(vector, inv_scale, cotangent, gain_vec):
    weighted = cotangent * gain_vec
    inner_mean = jnp.mean(weighted * vector, axis=-1, keepdims=True)
    return inv_scale * (weighted - vector * inv_scale * inv_scale * inner_mean)


def head_grads(
    query_in, key_input, value_input, grad_in, query_gain, key_gain, cos_tab, sin_tab, block_rows
):
    token_length, groups, per_group, head_dim = query_in.shape
    cos_four = cos_tab[:, None, None, :]
    sin_four = sin_tab[:, None, None, :]
    cos_three = cos_tab[:, None, :]
    sin_three = sin_tab[:, None, :]
    query_f = query_in.astype(jnp.float32)
    query_inv = inverse_rms(query_f)
    query_rot = rotate(query_f * query_inv * query_gain, cos_four, sin_four).astype(jnp.bfloat16)
    key_f = key_input.astype(jnp.float32)
    key_inv = inverse_rms(key_f)
    key_rot = rotate(key_f * key_inv * key_gain, cos_three, sin_three).astype(jnp.bfloat16)
    num_blocks = token_length // block_rows
    query_blocks = query_rot.reshape(num_blocks, block_rows, groups, per_group, head_dim)
    grad_blocks = grad_in.reshape(num_blocks, block_rows, groups, per_group, head_dim)

    def attend_block(carried, pieces):
        key_acc, value_acc = carried
        query_piece, grad_piece = pieces
        scores = product("qgrd,cgd->grqc", query_piece, key_rot) * score_scale
        row_max = jnp.max(scores, axis=-1, keepdims=True)
        shifted = jnp.exp(scores - row_max)
        attn_prob = shifted / jnp.sum(shifted, axis=-1, keepdims=True)
        prob_low = attn_prob.astype(jnp.bfloat16)
        prob_grad = product("qgrd,cgd->grqc", grad_piece, value_input)
        row_dot = jnp.sum(attn_prob * prob_grad, axis=-1, keepdims=True)
        score_grad = (attn_prob * (prob_grad - row_dot) * score_scale).astype(jnp.bfloat16)
        dq_piece = product("grqc,cgd->qgrd", score_grad, key_rot)
        key_acc = key_acc + product("grqc,qgrd->cgd", score_grad, query_piece)
        value_acc = value_acc + product("grqc,qgrd->cgd", prob_low, grad_piece)
        return ((key_acc, value_acc), dq_piece)

    empty_acc = jnp.zeros((token_length, groups, head_dim), jnp.float32)
    (key_rot_grad, value_acc), query_rot_grad = lax.scan(
        attend_block, (empty_acc, empty_acc), (query_blocks, grad_blocks)
    )
    query_rot_grad = query_rot_grad.reshape(token_length, groups, per_group, head_dim)
    query_grad = norm_back(
        query_f, query_inv, rotate_back(query_rot_grad, cos_four, sin_four), query_gain
    ).astype(jnp.bfloat16)
    key_portion = norm_back(
        key_f, key_inv, rotate_back(key_rot_grad, cos_three, sin_three), key_gain
    ).astype(jnp.bfloat16)
    return (query_grad, key_portion, value_acc.astype(jnp.bfloat16))


def on_device(
    inputs, queries, keys, values, out_grad, query_gain, key_gain, key_matrix, value_matrix
):
    sp_count = lax.axis_size("sp")
    dp_count = lax.axis_size("dp")
    token_row_block = inputs.shape[1]
    token_length = token_row_block * sp_count
    local_heads = QUERY_HEADS // sp_count
    portion_heads = min(local_heads, QUERY_HEADS // KEY_VALUE_HEADS)
    kv_here = local_heads // portion_heads
    group_copies = QUERY_HEADS // KEY_VALUE_HEADS // portion_heads
    key_value_width = KEY_VALUE_HEADS * HEAD_CHANNELS
    key_positions = jnp.repeat(
        keys[0].reshape(token_row_block, KEY_VALUE_HEADS, HEAD_CHANNELS), group_copies, axis=1
    ).reshape(token_row_block, key_value_width * group_copies)
    value_positions = jnp.repeat(
        values[0].reshape(token_row_block, KEY_VALUE_HEADS, HEAD_CHANNELS), group_copies, axis=1
    ).reshape(token_row_block, key_value_width * group_copies)
    grad_heads, query_heads, key_heads, value_heads = (
        lax.all_to_all(out_grad[0], "sp", split_axis=1, concat_axis=0, tiled=True),
        lax.all_to_all(queries[0], "sp", split_axis=1, concat_axis=0, tiled=True),
        lax.all_to_all(key_positions, "sp", split_axis=1, concat_axis=0, tiled=True),
        lax.all_to_all(value_positions, "sp", split_axis=1, concat_axis=0, tiled=True),
    )
    cos_tab, sin_tab = rotary_tables(token_length)
    query_part, key_portion, value_portion = head_grads(
        query_heads.reshape(token_length, kv_here, portion_heads, HEAD_CHANNELS),
        key_heads.reshape(token_length, kv_here, HEAD_CHANNELS),
        value_heads.reshape(token_length, kv_here, HEAD_CHANNELS),
        grad_heads.reshape(token_length, kv_here, portion_heads, HEAD_CHANNELS),
        query_gain,
        key_gain,
        cos_tab,
        sin_tab,
        min(512, token_length),
    )
    query_tokens, key_token_rows, value_token_rows = (
        lax.all_to_all(
            query_part.reshape(token_length, local_heads * HEAD_CHANNELS),
            "sp",
            split_axis=0,
            concat_axis=1,
            tiled=True,
        ),
        lax.all_to_all(
            key_portion.reshape(token_length, kv_here * HEAD_CHANNELS),
            "sp",
            split_axis=0,
            concat_axis=1,
            tiled=True,
        ),
        lax.all_to_all(
            value_portion.reshape(token_length, kv_here * HEAD_CHANNELS),
            "sp",
            split_axis=0,
            concat_axis=1,
            tiled=True,
        ),
    )
    key_gradient = (
        key_token_rows.reshape(token_row_block, KEY_VALUE_HEADS, group_copies, HEAD_CHANNELS)
        .astype(jnp.float32)
        .sum(axis=2)
        .astype(jnp.bfloat16)
    )
    value_gradient = (
        value_token_rows.reshape(token_row_block, KEY_VALUE_HEADS, group_copies, HEAD_CHANNELS)
        .astype(jnp.float32)
        .sum(axis=2)
        .astype(jnp.bfloat16)
    )
    projection_gradient = jnp.concatenate(
        [
            key_gradient.reshape(token_row_block, key_value_width),
            value_gradient.reshape(token_row_block, key_value_width),
        ],
        axis=1,
    )
    joined_weight = jnp.concatenate([key_matrix, value_matrix], axis=1)
    input_grad = lax.dot_general(
        projection_gradient,
        lax.all_gather(joined_weight, "dp", axis=0, tiled=True),
        (((1,), (1,)), ((), ())),
        preferred_element_type=jnp.float32,
    ).astype(jnp.bfloat16)
    token_in = inputs[0]
    width = inputs.shape[2]
    row_share = width // (sp_count * dp_count)
    permuted = (
        token_in.reshape(token_row_block, dp_count, sp_count, row_share)
        .transpose(0, 2, 1, 3)
        .reshape(token_row_block, width)
    )
    share_cols = lax.all_to_all(permuted, "sp", split_axis=1, concat_axis=0, tiled=True)
    all_grads = lax.all_gather(projection_gradient, "sp", axis=0, tiled=True)
    grad_piece = lax.psum_scatter(
        lax.dot_general(
            share_cols, all_grads, (((0,), (0,)), ((), ())), preferred_element_type=jnp.float32
        ).astype(jnp.bfloat16),
        "dp",
        scatter_dimension=0,
        tiled=True,
    ).astype(jnp.float32)
    weight_grad = lax.all_gather(grad_piece, "sp", axis=0, tiled=True)
    return (
        input_grad[None],
        query_tokens[None],
        weight_grad[:, :key_value_width],
        weight_grad[:, key_value_width:],
    )


LANES = 128
VMEM_BYTES = 67043328
MESH = pl.DeviceIdType.MESH
F32 = jnp.float32
BF16 = jnp.bfloat16


def pair_tables(token_length):
    position = np.arange(token_length)
    half_pairs = HEAD_CHANNELS // 4
    inv_freq = (rope_base ** (-np.arange(half_pairs) / half_pairs)).astype(np.float32)
    row = (position // GRID).astype(np.float32)
    col = (position % GRID).astype(np.float32)
    angles = np.concatenate([row[:, None] * inv_freq, col[:, None] * inv_freq], axis=1)
    cos_tab = np.repeat(np.cos(angles), 2, axis=1)
    sin_tab = np.repeat(np.sin(angles), 2, axis=1)
    sin_tab[:, 0::2] *= -1.0
    return (
        np.tile(cos_tab, (1, 2)).astype(np.float32),
        np.tile(sin_tab, (1, 2)).astype(np.float32),
    )


def swap_pairs(x):
    lane = lax.broadcasted_iota(jnp.int32, x.shape, 1)
    return jnp.where(lane % 2 == 0, pltpu.roll(x, LANES - 1, 1), pltpu.roll(x, 1, 1))


def head_mean(z):
    row = lax.broadcasted_iota(jnp.int32, (LANES, LANES), 0) // HEAD_CHANNELS
    col = lax.broadcasted_iota(jnp.int32, (LANES, LANES), 1) // HEAD_CHANNELS
    ones = jnp.where(row == col, 1.0, 0.0).astype(BF16)
    high = z.astype(BF16)
    low = (z - high.astype(F32)).astype(BF16)
    total = jnp.dot(high, ones, preferred_element_type=F32)
    total = total + jnp.dot(low, ones, preferred_element_type=F32)
    return total * (1.0 / HEAD_CHANNELS)


def norm_rotate(x, gain, cos_tab, sin_tab):
    inv = lax.rsqrt(head_mean(x * x) + norm_eps)
    y = x * inv * gain
    return y * cos_tab + swap_pairs(y) * sin_tab


def norm_rotate_back(x, cotangent, gain, cos_tab, sin_tab):
    turned = cotangent * cos_tab - swap_pairs(cotangent) * sin_tab
    inv = lax.rsqrt(head_mean(x * x) + norm_eps)
    weighted = turned * gain
    return inv * (weighted - x * (inv * inv * head_mean(weighted * x)))


def contract(a, b, dims):
    return lax.dot_general(a, b, (dims, ((), ())), preferred_element_type=F32)


def step_kernel(
    n, dp,
    x_hbm, q_hbm, k_hbm, v_hbm, do_hbm, qg_hbm, kg_hbm, km_hbm, vm_hbm, cos_hbm, sin_hbm,
    dx_buf, dq_buf, kw_buf, vw_buf,
    qg_ref, kg_ref, q_buf, do_buf, cos_buf, sin_buf, k_all, v_all, x_all, wk_all, wv_all,
    q_st, do_st, k_st, v_st, dq_acc, part, got, g_all, x_t, wg_part, wg_got,
    fin_all,
    local_sem, kv_send, kv_recv, x_send, x_recv, w_send, w_recv, w_fsend,
    p_send, p_recv, g_send, g_recv, g_fsend, r_send, r_recv, f_send, f_recv,
):
    me = lax.axis_index("sp")
    md = lax.axis_index("dp")
    rows, q_width = q_buf.shape
    head_pairs = k_all.shape[0]
    share = x_all.shape[2]
    per_group = q_width // (2 * head_pairs * HEAD_CHANNELS)
    mate = md + 1 - 2 * (md % 2)
    piece = share // n

    def sp_peer(o):
        return lax.rem(me + o, n)

    def sp_from(o):
        return lax.rem(me - o + n, n)

    def dp_peer(o):
        return lax.rem(md + o, dp)

    def dp_from(o):
        return lax.rem(md - o + dp, dp)

    def mate_from(o):
        return lax.rem(mate - o + dp, dp)

    def pair(c):
        return pl.ds(c * LANES, LANES)

    barrier = pltpu.get_barrier_semaphore()
    for o in range(1, n):
        pl.semaphore_signal(barrier, inc=1, device_id={"sp": sp_peer(o)}, device_id_type=MESH)
    for o in range(1, dp):
        pl.semaphore_signal(barrier, inc=1, device_id={"dp": dp_peer(o)}, device_id_type=MESH)

    def columns(d):
        return pl.ds(pl.multiple_of(d * share, share), share)

    wanted = [
        (q_hbm, q_buf), (do_hbm, do_buf), (cos_hbm, cos_buf), (sin_hbm, sin_buf),
        (x_hbm.at[:, columns(md)], x_all.at[md]),
        (km_hbm, wk_all.at[md]), (vm_hbm, wv_all.at[md]), (qg_hbm, qg_ref), (kg_hbm, kg_ref),
    ]
    for c in range(head_pairs):
        wanted.append((k_hbm.at[:, pair(c)], k_all.at[c, me]))
        wanted.append((v_hbm.at[:, pair(c)], v_all.at[c, me]))
    local = [
        pltpu.make_async_copy(src, dst, local_sem.at[i]) for i, (src, dst) in enumerate(wanted)
    ]
    for copy in local:
        copy.start()

    def remote(src, dst, send, recv, where):
        return pltpu.make_async_remote_copy(
            src_ref=src, dst_ref=dst, send_sem=send, recv_sem=recv,
            device_id=where, device_id_type=MESH,
        )

    pl.semaphore_wait(barrier, n + dp - 2)

    sends = []

    def send(*args):
        copy = remote(*args)
        copy.start()
        sends.append(copy)

    def arrived(dst, recv):
        remote(dst, dst, recv, recv, {"sp": me}).wait_recv()

    order = sorted(range(1, n), key=lambda o: -min(o, n - o))
    for c in range(head_pairs):
        for kind, (src, dst) in enumerate([(k_hbm, k_all), (v_hbm, v_all)]):
            for o in order:
                send(src.at[:, pair(c)], dst.at[c, me], kv_send.at[kind, c, o],
                     kv_recv.at[kind, c, me], {"sp": sp_peer(o)})
    weights = [(km_hbm, wk_all), (vm_hbm, wv_all)]
    for kind, (src, dst) in enumerate(weights):
        for o in range(2, dp, 2):
            send(src, dst.at[md], w_send.at[kind, o], w_recv.at[kind, md], {"dp": dp_peer(o)})
        send(src, dst.at[md], w_send.at[kind, 1], w_recv.at[kind, md], {"dp": mate})
    for o in range(1, dp):
        send(x_hbm.at[:, columns(dp_peer(o))], x_all.at[md], x_send.at[o], x_recv.at[md],
             {"dp": dp_peer(o)})

    for copy in local:
        copy.wait()

    my_rows = pl.ds(pl.multiple_of(me * rows, rows), rows)
    cos_own = cos_buf[my_rows, :]
    sin_own = sin_buf[my_rows, :]
    q_gain = jnp.concatenate([qg_ref[...], qg_ref[...]], axis=1)
    k_gain = jnp.concatenate([kg_ref[...], kg_ref[...]], axis=1)

    for c in range(q_width // LANES):
        turned = norm_rotate(q_buf[:, pair(c)].astype(F32), q_gain, cos_own, sin_own).astype(BF16)
        grads = do_buf[:, pair(c)]
        for a in range(2):
            h = 2 * c + a
            to = pl.ds((h % per_group) * rows, rows)
            half = slice(a * HEAD_CHANNELS, (a + 1) * HEAD_CHANNELS)
            q_st[h // per_group, to, :] = turned[:, half]
            do_st[h // per_group, to, :] = grads[:, half]

    def stack_keys(c, src):
        at = pl.ds(pl.multiple_of(src * rows, rows), rows)
        turned = norm_rotate(
            k_all[c, src].astype(F32), k_gain, cos_buf[at, :], sin_buf[at, :]
        ).astype(BF16)
        vals = v_all[c, src]
        for a in range(2):
            half = slice(a * HEAD_CHANNELS, (a + 1) * HEAD_CHANNELS)
            k_st[2 * c + a, at, :] = turned[:, half]
            v_st[2 * c + a, at, :] = vals[:, half]

    def attend(g):
        qs = q_st[g]
        dos = do_st[g]
        ks = k_st[g]
        vs = v_st[g]
        scores = contract(ks, qs, ((1,), (1,))) * score_scale
        shifted = jnp.exp(scores - jnp.max(scores, axis=0, keepdims=True))
        prob = shifted * (1.0 / jnp.sum(shifted, axis=0, keepdims=True))
        value_part = contract(prob.astype(BF16), dos, ((1,), (0,)))
        prob_grad = contract(vs, dos, ((1,), (1,)))
        row_dot = jnp.sum(prob * prob_grad, axis=0, keepdims=True)
        score_grad = (prob * (prob_grad - row_dot) * score_scale).astype(BF16)
        key_part = contract(score_grad, qs, ((1,), (0,)))
        dq_t = contract(ks, score_grad, ((0,), (0,)))
        for r in range(0, per_group, 2):
            both = jnp.concatenate(
                [dq_t[:, r * rows:(r + 1) * rows], dq_t[:, (r + 1) * rows:(r + 2) * rows]], axis=0
            )
            head = g * per_group + r
            dq_acc[:, head * HEAD_CHANNELS:head * HEAD_CHANNELS + LANES] = both.T
        return key_part, value_part

    for c in range(head_pairs):
        stack_keys(c, me)
    for c in range(head_pairs):
        for o in range(1, n):
            src = sp_from(o)
            arrived(k_all.at[c, src], kv_recv.at[0, c, src])
            arrived(v_all.at[c, src], kv_recv.at[1, c, src])
            stack_keys(c, src)
        key_low, value_low = attend(2 * c)
        key_high, value_high = attend(2 * c + 1)
        both = jnp.concatenate([key_low, key_high, value_low, value_high], axis=1).astype(BF16)
        for j in range(n):
            part[c, j] = both[j * rows:(j + 1) * rows, :]
        for o in order:
            send(part.at[c, sp_peer(o)], got.at[c, me], p_send.at[c, o], p_recv.at[c, me],
                 {"sp": sp_peer(o)})

    def own_grads(c):
        total = part[c, me].astype(F32)
        for o in range(1, n):
            src = sp_from(o)
            arrived(got.at[c, src], p_recv.at[c, src])
            total = total + got[c, src].astype(F32)
        g_all[c, md, :, :LANES] = norm_rotate_back(
            k_all[c, me].astype(F32), total[:, :LANES], k_gain, cos_own, sin_own
        ).astype(BF16)
        g_all[c, md, :, LANES:] = total[:, LANES:].astype(BF16)
        mine = g_all.at[c, md]
        for o in range(2, dp, 2):
            send(mine, mine, g_send.at[c, o], g_recv.at[c, md], {"dp": dp_peer(o)})
        send(mine, mine, g_send.at[c, 1], g_recv.at[c, md], {"dp": mate})

    def pass_on(c):
        for o in range(2, dp, 2):
            src = dp_from(o)
            theirs = g_all.at[c, src]
            arrived(theirs, g_recv.at[c, src])
            send(theirs, theirs, g_fsend.at[c, o], g_recv.at[c, src], {"dp": mate})

    def weight_grads(c):
        total = contract(x_t[md], g_all[c, md], ((1,), (0,)))
        for o in range(2, dp, 2):
            src = dp_from(o)
            total = total + contract(x_t[src], g_all[c, src], ((1,), (0,)))
        for o in range(0, dp, 2):
            src = mate_from(o)
            arrived(g_all.at[c, src], g_recv.at[c, src])
            total = total + contract(x_t[src], g_all[c, src], ((1,), (0,)))
        for j in range(n):
            wg_part[c, j] = total[j * piece:(j + 1) * piece, :].astype(BF16)
        for o in order:
            send(wg_part.at[c, sp_peer(o)], wg_got.at[c, me], r_send.at[c, o], r_recv.at[c, me],
                 {"sp": sp_peer(o)})

    def sum_weight_grads(c):
        total = wg_part[c, me].astype(F32)
        for o in range(1, n):
            src = sp_from(o)
            arrived(wg_got.at[c, src], r_recv.at[c, src])
            total = total + wg_got[c, src].astype(F32)
        fin_all[c, me] = total.astype(BF16)
        mine = fin_all.at[c, me]
        for o in order:
            send(mine, mine, f_send.at[c, o], f_recv.at[c, me], {"sp": sp_peer(o)})

    for o in range(dp):
        src = dp_from(o)
        if o:
            arrived(x_all.at[src], x_recv.at[src])
        x_t[src] = x_all[src].T

    for c in range(head_pairs):
        own_grads(c)
        if c == 0:
            for kind, (_, dst) in enumerate(weights):
                for o in range(2, dp, 2):
                    src = dp_from(o)
                    arrived(dst.at[src], w_recv.at[kind, src])
                    send(dst.at[src], dst.at[src], w_fsend.at[kind, o], w_recv.at[kind, src],
                         {"dp": mate})
            for i in range(q_width // LANES):
                dq_buf[:, pair(i)] = norm_rotate_back(
                    q_buf[:, pair(i)].astype(F32), dq_acc[:, pair(i)], q_gain, cos_own, sin_own
                ).astype(BF16)

    own = jnp.concatenate(
        [g_all[c, md, :, :LANES] for c in range(head_pairs)]
        + [g_all[c, md, :, LANES:] for c in range(head_pairs)], axis=1)
    kv_width = head_pairs * LANES

    def project(src):
        out = contract(own[:, :kv_width], wk_all[src], ((1,), (1,)))
        out = out + contract(own[:, kv_width:], wv_all[src], ((1,), (1,)))
        dx_buf[:, columns(src)] = out.astype(BF16)

    for c in range(head_pairs):
        pass_on(c)
        weight_grads(c)
    for o in range(0, dp, 2):
        project(dp_from(o))
    for o in range(0, dp, 2):
        src = mate_from(o)
        for kind, (_, dst) in enumerate(weights):
            arrived(dst.at[src], w_recv.at[kind, src])
        project(src)
    for c in range(head_pairs):
        sum_weight_grads(c)
    for c in range(head_pairs):
        for o in range(n):
            src = sp_from(o)
            if o:
                arrived(fin_all.at[c, src], f_recv.at[c, src])
            at = pl.ds(pl.multiple_of(src * piece, piece), piece)
            kw_buf[at, pair(c)] = fin_all[c, src, :, :LANES].astype(F32)
            vw_buf[at, pair(c)] = fin_all[c, src, :, LANES:].astype(F32)
    for copy in sends:
        copy.wait_send()


def write_kernel(*refs):
    count = (len(refs) - 1) // 2
    copies = [
        pltpu.make_async_copy(refs[i], refs[count + i], refs[-1].at[i]) for i in range(count)
    ]
    for copy in copies:
        copy.start()
    for copy in copies:
        copy.wait()


def kernel_step(
    n, dp, inputs, queries, keys, values, out_grad, query_gain, key_gain, key_matrix, value_matrix
):
    rows, width = inputs.shape[1:]
    q_width = queries.shape[2]
    kv_width = keys.shape[2]
    length = rows * n
    share = width // dp
    kv_heads = kv_width // HEAD_CHANNELS
    half = kv_heads // 2
    stack = rows * (q_width // kv_width)
    cos_tab, sin_tab = pair_tables(length)
    vmem = pltpu.VMEM
    dma = pltpu.SemaphoreType.DMA
    wide = 2 * LANES
    scratch = [
        vmem((1, HEAD_CHANNELS), F32), vmem((1, HEAD_CHANNELS), F32),
        vmem((rows, q_width), BF16), vmem((rows, q_width), BF16),
        vmem((length, LANES), F32), vmem((length, LANES), F32),
        vmem((half, n, rows, LANES), BF16), vmem((half, n, rows, LANES), BF16),
        vmem((dp, rows, share), BF16),
        vmem((dp, share, kv_width), BF16), vmem((dp, share, kv_width), BF16),
        vmem((kv_heads, stack, HEAD_CHANNELS), BF16), vmem((kv_heads, stack, HEAD_CHANNELS), BF16),
        vmem((kv_heads, length, HEAD_CHANNELS), BF16), vmem((kv_heads, length, HEAD_CHANNELS), BF16),
        vmem((rows, q_width), F32),
        vmem((half, n, rows, wide), BF16), vmem((half, n, rows, wide), BF16),
        vmem((half, dp, rows, wide), BF16), vmem((dp, share, rows), BF16),
        vmem((half, n, share // n, wide), BF16), vmem((half, n, share // n, wide), BF16),
        vmem((half, n, share // n, wide), BF16),
        dma((9 + 2 * half,)),
        dma((2, half, n)), dma((2, half, n)), dma((dp,)), dma((dp,)),
        dma((2, dp)), dma((2, dp)), dma((2, dp)),
        dma((half, n)), dma((half, n)),
        dma((half, dp)), dma((half, dp)), dma((half, dp)),
        dma((half, n)), dma((half, n)), dma((half, n)), dma((half, n)),
    ]
    hbm = pl.BlockSpec(memory_space=pltpu.HBM)
    here = pl.BlockSpec(memory_space=pltpu.VMEM)
    results = [
        ((rows, width), BF16), ((rows, q_width), BF16),
        ((share, kv_width), F32), ((share, kv_width), F32),
    ]
    held_bytes = 65536 + sum(a * b * jnp.dtype(kind).itemsize for (a, b), kind in results)
    held = pl.pallas_call(
        functools.partial(step_kernel, n, dp),
        out_shape=[pltpu.VMEM(shape, kind) for shape, kind in results],
        in_specs=[hbm] * 11,
        out_specs=[here] * 4,
        scratch_shapes=scratch,
        compiler_params=pltpu.CompilerParams(
            collective_id=0, has_side_effects=True, vmem_limit_bytes=VMEM_BYTES - held_bytes
        ),
    )(
        inputs[0], queries[0], keys[0], values[0], out_grad[0],
        query_gain[None], key_gain[None],
        key_matrix, value_matrix, jnp.asarray(cos_tab), jnp.asarray(sin_tab),
    )
    dx, dq, kw, vw = pl.pallas_call(
        write_kernel,
        out_shape=[jax.ShapeDtypeStruct(shape, kind) for shape, kind in results],
        in_specs=[here] * 4,
        out_specs=[hbm] * 4,
        scratch_shapes=[dma((4,))],
        compiler_params=pltpu.CompilerParams(vmem_limit_bytes=8 * 1024 * 1024),
    )(*held)
    return dx[None], dq[None], kw, vw


def device_step(inputs, *rest):
    n = lax.axis_size("sp")
    dp = lax.axis_size("dp")
    rows, width = inputs.shape[1:]
    fits = dp % 2 == 0 and width % (dp * LANES) == 0 and rows % LANES == 0 and rows * n <= 1024
    if fits and (width // dp) % (16 * n) == 0:
        return kernel_step(n, dp, inputs, *rest)
    return on_device(inputs, *rest)


def solution(mesh):
    return jax.shard_map(
        device_step,
        mesh=mesh,
        in_specs=(
            P("dp", "sp", None),
            P("dp", "sp", None),
            P("dp", "sp", None),
            P("dp", "sp", None),
            P("dp", "sp", None),
            P(),
            P(),
            P("dp", None),
            P("dp", None),
        ),
        out_specs=(P("dp", "sp", None), P("dp", "sp", None), P("dp", None), P("dp", None)),
        check_vma=False,
    )
```

profile of v0, /device:TPU:0, one launch (start us, length us, event | category | flops | bytes accessed | tf_op | source)
XLA Modules:
  0.0 49.3 jit_solution(6496725561633461637)
XLA Ops:
  0.6 47.5 %shard_map.138 = (bf16[128,2048]{1,0:T(8,128)(2,1)S(1)}, bf16[128,1024]{1,0:T(8,128)(2,1)S(1)}, f32[256,256]{1,0:T(8,128)S(1)}, f32[256,256]{1,0:T(8,128)S(1)}) custom-call(bf16[128,2048]{1,0:T(8,128)(2,1)} %bitcast.9, bf16[128,1024]{1,0:T(8,128)(2,1)} %bitcast.10, bf16[128,256]{1,0:T(8,128)(2,1)} %bitcast.12, bf16[128,256]{1,0:T(8,128)(2,1)} %bitcast.13, ...), custom_call_target="tpu_custom_call" | custom-call | tf_op jit(solution)/shard_map/pallas_call | solution.py:600
  48.2 1.1 %shard_map.139 = (bf16[128,2048]{1,0:T(8,128)(2,1)}, bf16[128,1024]{1,0:T(8,128)(2,1)}, f32[256,256]{1,0:T(8,128)}, f32[256,256]{1,0:T(8,128)}) custom-call(bf16[128,2048]{1,0:T(8,128)(2,1)S(1)} %get-tuple-element.12.refs_0_, bf16[128,1024]{1,0:T(8,128)(2,1)S(1)} %get-tuple-element.13.refs_1_, f32[256,256]{1,0:T(8,128)S(1)} %get-tuple-element.14.refs_2_, ...), custom_call_target="tpu_custom_call" | custom-call | tf_op jit(solution)/shard_map/pallas_call | solution.py:614
where the time goes:
time: 49.4 us; the launch traced here: 49.3 us
  Pallas kernels  48.6 us (98%)
  between operations  0.64 us (1%)
    pallas_call x1, Pallas kernels, kernel_step(): pl.pallas_call(functools.partial(step_kernel, n, dp), out_shape=[pltpu.VM...  47.5 us
    pallas_call x1, Pallas kernels, kernel_step(): pl.pallas_call(write_kernel, out_shape=[jax.ShapeDtypeStruct(shape, kind)...  1.09 us

commit v1 on v0

--- a/solution.py
+++ b/solution.py
@@ -265,12 +265,11 @@
 def norm_rotate(x, gain, cos_tab, sin_tab):
     inv = lax.rsqrt(head_mean(x * x) + norm_eps)
     y = x * inv * gain
-    return y * cos_tab + swap_pairs(y) * sin_tab
-
-
-def norm_rotate_back(x, cotangent, gain, cos_tab, sin_tab):
+    return y * cos_tab + swap_pairs(y) * sin_tab, inv
+
+
+def norm_rotate_back(x, inv, cotangent, gain, cos_tab, sin_tab):
     turned = cotangent * cos_tab - swap_pairs(cotangent) * sin_tab
-    inv = lax.rsqrt(head_mean(x * x) + norm_eps)
     weighted = turned * gain
     return inv * (weighted - x * (inv * inv * head_mean(weighted * x)))
 
@@ -283,20 +282,28 @@
     n, dp,
     x_hbm, q_hbm, k_hbm, v_hbm, do_hbm, qg_hbm, kg_hbm, km_hbm, vm_hbm, cos_hbm, sin_hbm,
     dx_buf, dq_buf, kw_buf, vw_buf,
-    qg_ref, kg_ref, q_buf, do_buf, cos_buf, sin_buf, k_all, v_all, x_all, wk_all, wv_all,
-    q_st, do_st, k_st, v_st, dq_acc, part, got, g_all, x_t, wg_part, wg_got,
-    fin_all,
-    local_sem, kv_send, kv_recv, x_send, x_recv, w_send, w_recv, w_fsend,
-    p_send, p_recv, g_send, g_recv, g_fsend, r_send, r_recv, f_send, f_recv,
+    qg_ref, kg_ref, q_buf, do_buf, cos_buf, sin_buf, k_own, v_own, k_head, kv_all, q_inv, q_st, do_st,
+    x_all, x_t, wk_all, wv_all, dq_acc, part, comb_in, comb, got, g_all, own_k, own_v,
+    wg_part, wg_got, fin_all,
+    local_sem, kv_send, kv_recv, x_sem, w_send, w_recv, p_send, c_recv, p_recv,
+    g_send, gd_recv, gm_recv, r_send, r_recv, f_recv,
 ):
     me = lax.axis_index("sp")
     md = lax.axis_index("dp")
     rows, q_width = q_buf.shape
-    head_pairs = k_all.shape[0]
+    heads = kv_all.shape[1]
     share = x_all.shape[2]
-    per_group = q_width // (2 * head_pairs * HEAD_CHANNELS)
+    per_group = q_width // (heads * HEAD_CHANNELS)
+    half_share = share // 2
     mate = md + 1 - 2 * (md % 2)
     piece = share // n
+    last = n - 1
+    partner = me + 1 - 2 * (me % 2)
+    low_side = me < n // 2
+    other_end = jnp.where(low_side, last, 0)
+    other_mid = jnp.where(low_side, n // 2, n // 2 - 1)
+    is_end = jnp.logical_or(me == 0, me == last)
+    near_chips = dp // 2 - 1
 
     def sp_peer(o):
         return lax.rem(me + o, n)
@@ -316,23 +323,36 @@
     def pair(c):
         return pl.ds(c * LANES, LANES)
 
-    barrier = pltpu.get_barrier_semaphore()
-    for o in range(1, n):
-        pl.semaphore_signal(barrier, inc=1, device_id={"sp": sp_peer(o)}, device_id_type=MESH)
-    for o in range(1, dp):
-        pl.semaphore_signal(barrier, inc=1, device_id={"dp": dp_peer(o)}, device_id_type=MESH)
-
     def columns(d):
         return pl.ds(pl.multiple_of(d * share, share), share)
 
+    barrier = pltpu.get_barrier_semaphore()
+
+    def greet(where):
+        pl.semaphore_signal(barrier, inc=1, device_id=where, device_id_type=MESH)
+
+    @pl.when(me > 0)
+    def _():
+        greet({"sp": me - 1})
+
+    @pl.when(me < last)
+    def _():
+        greet({"sp": me + 1})
+
+    @pl.when(me == 0)
+    def _():
+        greet({"sp": last})
+
+    for o in range(1, dp):
+        greet({"dp": dp_peer(o)})
+
+    my_rows = pl.ds(pl.multiple_of(me * rows, rows), rows)
     wanted = [
-        (q_hbm, q_buf), (do_hbm, do_buf), (cos_hbm, cos_buf), (sin_hbm, sin_buf),
-        (x_hbm.at[:, columns(md)], x_all.at[md]),
-        (km_hbm, wk_all.at[md]), (vm_hbm, wv_all.at[md]), (qg_hbm, qg_ref), (kg_hbm, kg_ref),
+        (k_hbm, k_own), (v_hbm, v_own), (cos_hbm.at[my_rows, :], cos_buf),
+        (sin_hbm.at[my_rows, :], sin_buf), (kg_hbm, kg_ref), (qg_hbm, qg_ref),
+        (q_hbm, q_buf), (do_hbm, do_buf),
+        (x_hbm.at[:, columns(md)], x_all.at[md]), (km_hbm, wk_all.at[md]), (vm_hbm, wv_all.at[md]),
     ]
-    for c in range(head_pairs):
-        wanted.append((k_hbm.at[:, pair(c)], k_all.at[c, me]))
-        wanted.append((v_hbm.at[:, pair(c)], v_all.at[c, me]))
     local = [
         pltpu.make_async_copy(src, dst, local_sem.at[i]) for i, (src, dst) in enumerate(wanted)
     ]
@@ -345,202 +365,334 @@
             device_id=where, device_id_type=MESH,
         )
 
-    pl.semaphore_wait(barrier, n + dp - 2)
-
-    sends = []
-
     def send(*args):
-        copy = remote(*args)
-        copy.start()
-        sends.append(copy)
+        remote(*args).start()
 
     def arrived(dst, recv):
         remote(dst, dst, recv, recv, {"sp": me}).wait_recv()
 
-    order = sorted(range(1, n), key=lambda o: -min(o, n - o))
-    for c in range(head_pairs):
-        for kind, (src, dst) in enumerate([(k_hbm, k_all), (v_hbm, v_all)]):
-            for o in order:
-                send(src.at[:, pair(c)], dst.at[c, me], kv_send.at[kind, c, o],
-                     kv_recv.at[kind, c, me], {"sp": sp_peer(o)})
-    weights = [(km_hbm, wk_all), (vm_hbm, wv_all)]
-    for kind, (src, dst) in enumerate(weights):
-        for o in range(2, dp, 2):
-            send(src, dst.at[md], w_send.at[kind, o], w_recv.at[kind, md], {"dp": dp_peer(o)})
-        send(src, dst.at[md], w_send.at[kind, 1], w_recv.at[kind, md], {"dp": mate})
-    for o in range(1, dp):
-        send(x_hbm.at[:, columns(dp_peer(o))], x_all.at[md], x_send.at[o], x_recv.at[md],
-             {"dp": dp_peer(o)})
-
-    for copy in local:
-        copy.wait()
-
-    my_rows = pl.ds(pl.multiple_of(me * rows, rows), rows)
-    cos_own = cos_buf[my_rows, :]
-    sin_own = sin_buf[my_rows, :]
+    def departed(src, sem):
+        remote(src, src, sem, sem, {"sp": me}).wait_send()
+
+    low_lanes = lax.broadcasted_iota(jnp.int32, (rows, LANES), 1) < HEAD_CHANNELS
+
+    def shift(a):
+        return pltpu.roll(a, HEAD_CHANNELS, 1)
+
+    with jax.named_scope("local"):
+        for copy in local[:6]:
+            copy.wait()
+    cos_own = cos_buf[...]
+    sin_own = sin_buf[...]
     q_gain = jnp.concatenate([qg_ref[...], qg_ref[...]], axis=1)
     k_gain = jnp.concatenate([kg_ref[...], kg_ref[...]], axis=1)
 
-    for c in range(q_width // LANES):
-        turned = norm_rotate(q_buf[:, pair(c)].astype(F32), q_gain, cos_own, sin_own).astype(BF16)
-        grads = do_buf[:, pair(c)]
-        for a in range(2):
-            h = 2 * c + a
-            to = pl.ds((h % per_group) * rows, rows)
-            half = slice(a * HEAD_CHANNELS, (a + 1) * HEAD_CHANNELS)
-            q_st[h // per_group, to, :] = turned[:, half]
-            do_st[h // per_group, to, :] = grads[:, half]
-
-    def stack_keys(c, src):
-        at = pl.ds(pl.multiple_of(src * rows, rows), rows)
-        turned = norm_rotate(
-            k_all[c, src].astype(F32), k_gain, cos_buf[at, :], sin_buf[at, :]
-        ).astype(BF16)
-        vals = v_all[c, src]
-        for a in range(2):
-            half = slice(a * HEAD_CHANNELS, (a + 1) * HEAD_CHANNELS)
-            k_st[2 * c + a, at, :] = turned[:, half]
-            v_st[2 * c + a, at, :] = vals[:, half]
+    for c in range(heads // 2):
+        keys = k_own[:, pair(c)].astype(F32)
+        vals = v_own[:, pair(c)].astype(F32)
+        turned = norm_rotate(keys, k_gain, cos_own, sin_own)[0]
+        kv_all[me, 2 * c] = jnp.where(low_lanes, turned, shift(vals)).astype(BF16)
+        kv_all[me, 2 * c + 1] = jnp.where(low_lanes, shift(turned), vals).astype(BF16)
+        k_head[2 * c] = keys
+        k_head[2 * c + 1] = shift(keys)
+
+    with jax.named_scope("barrier"):
+        pl.semaphore_wait(
+            barrier, dp - 1 + jnp.where(me > 0, 1, 0) + jnp.where(me < last, 1, 0)
+            + jnp.where(me == last, 1, 0)
+        )
+
+    def send_kv(src, g, sem, where):
+        block = kv_all.at[src, g]
+        send(block, block, kv_send.at[sem], kv_recv.at[src, g], {"sp": where})
+
+    for g in range(heads):
+        @pl.when(me < last)
+        def _():
+            send_kv(me, g, 0, me + 1)
+
+        @pl.when(me > 0)
+        def _():
+            send_kv(me, g, 1, me - 1)
+
+        @pl.when(me == last)
+        def _():
+            send_kv(me, g, 2, 0)
+
+    for o in range(1, dp):
+        send(x_hbm.at[:, columns(dp_peer(o))], x_all.at[md], x_sem.at[0], x_sem.at[1],
+             {"dp": dp_peer(o)})
+
+    top = pl.ds(0, half_share)
+    bottom = pl.ds(half_share, half_share)
+    full = pl.ds(0, share)
+    weights = [(km_hbm, wk_all, full), (vm_hbm, wv_all, top), (vm_hbm, wv_all, bottom)]
+
+    def send_weights(kind):
+        src, dst, at = weights[kind]
+        for o in range(2, dp, 2):
+            send(src.at[at], dst.at[md, at], w_send.at[kind], w_recv.at[kind, 0],
+                 {"dp": dp_peer(o)})
+        send(src.at[at], dst.at[md, at], w_send.at[kind], w_recv.at[kind, 1], {"dp": mate})
+
+    def pass_weights(kind):
+        _, dst, at = weights[kind]
+        arrived(dst.at[pl.ds(0, near_chips), at], w_recv.at[kind, 0])
+        for o in range(2, dp, 2):
+            block = dst.at[dp_from(o), at]
+            send(block, block, w_send.at[kind], w_recv.at[kind, 1], {"dp": mate})
+
+    def finish_weights(kind):
+        _, dst, at = weights[kind]
+        arrived(dst.at[pl.ds(0, dp // 2), at], w_recv.at[kind, 1])
+
+    send_weights(0)
+    send_weights(1)
+
+    with jax.named_scope("local2"):
+        for copy in local[6:8]:
+            copy.wait()
+    with jax.named_scope("qrot"):
+        for c in range(q_width // LANES):
+            turned, inv = norm_rotate(q_buf[:, pair(c)].astype(F32), q_gain, cos_own, sin_own)
+            q_inv[:, pair(c)] = inv
+            turned = turned * score_scale
+            grads = do_buf[:, pair(c)].astype(F32)
+            g, r = divmod(2 * c, per_group)
+            for a, (query, grad) in enumerate([(turned, shift(grads)), (shift(turned), grads)]):
+                to = pl.ds((r + a) * rows, rows)
+                q_st[g, to, :] = jnp.where(low_lanes, query, 0.0).astype(BF16)
+                do_st[g, to, :] = jnp.where(low_lanes, 0.0, grad).astype(BF16)
+
+    def take_kv(src, g):
+        arrived(kv_all.at[src, g], kv_recv.at[src, g])
+
+    def relay(src, g, where):
+        take_kv(src, g)
+        send_kv(src, g, 3 + src, where)
+
+    with jax.named_scope("relay"):
+        @pl.when(me == 1)
+        def _():
+            for g in range(heads + 2):
+                if g < heads:
+                    relay(0, g, 2)
+                if g >= 2:
+                    relay(2, g - 2, 0)
+
+        @pl.when(me == 2)
+        def _():
+            for g in range(heads):
+                relay(1, g, 3)
+                if g < 2:
+                    relay(3, g, 1)
+                relay(0, g, 3)
 
     def attend(g):
-        qs = q_st[g]
-        dos = do_st[g]
-        ks = k_st[g]
-        vs = v_st[g]
-        scores = contract(ks, qs, ((1,), (1,))) * score_scale
+        kv = kv_all[:, g].reshape(n * rows, LANES)
+        queries = q_st[g]
+        grads = do_st[g]
+        scores = contract(kv, queries, ((1,), (1,)))
         shifted = jnp.exp(scores - jnp.max(scores, axis=0, keepdims=True))
         prob = shifted * (1.0 / jnp.sum(shifted, axis=0, keepdims=True))
-        value_part = contract(prob.astype(BF16), dos, ((1,), (0,)))
-        prob_grad = contract(vs, dos, ((1,), (1,)))
+        prob_grad = contract(kv, grads, ((1,), (1,)))
         row_dot = jnp.sum(prob * prob_grad, axis=0, keepdims=True)
-        score_grad = (prob * (prob_grad - row_dot) * score_scale).astype(BF16)
-        key_part = contract(score_grad, qs, ((1,), (0,)))
-        dq_t = contract(ks, score_grad, ((0,), (0,)))
+        score_grad = (prob * (prob_grad - row_dot)).astype(BF16)
+        both = contract(score_grad, queries, ((1,), (0,)))
+        both = both + contract(prob.astype(BF16), grads, ((1,), (0,)))
+        part[g] = both.astype(BF16).reshape(n, rows, LANES)
+        return kv, score_grad
+
+    def query_part(g, kv, score_grad):
+        dq_t = contract(kv[:, :HEAD_CHANNELS], score_grad, ((0,), (0,)))
         for r in range(0, per_group, 2):
-            both = jnp.concatenate(
+            turned = jnp.concatenate(
                 [dq_t[:, r * rows:(r + 1) * rows], dq_t[:, (r + 1) * rows:(r + 2) * rows]], axis=0
             )
             head = g * per_group + r
-            dq_acc[:, head * HEAD_CHANNELS:head * HEAD_CHANNELS + LANES] = both.T
-        return key_part, value_part
-
-    for c in range(head_pairs):
-        stack_keys(c, me)
-    for c in range(head_pairs):
+            dq_acc[:, head * HEAD_CHANNELS:head * HEAD_CHANNELS + LANES] = turned.T
+
+    def send_parts(g):
+        @pl.when(is_end)
+        def _():
+            send(part.at[g, other_end], comb_in.at[g, 0], p_send.at[0], c_recv.at[g, 0],
+                 {"sp": partner})
+            send(part.at[g, other_mid], comb_in.at[g, 1], p_send.at[0], c_recv.at[g, 1],
+                 {"sp": partner})
+
+        send(part.at[g, partner], got.at[g, 0], p_send.at[0], p_recv.at[g], {"sp": partner})
+
+    def combine(g):
+        @pl.when(jnp.logical_not(is_end))
+        def _():
+            for i, where in enumerate([other_end, other_mid]):
+                arrived(comb_in.at[g, i], c_recv.at[g, i])
+                total = comb_in[g, i].astype(F32) + part[g, where].astype(F32)
+                comb[g, i] = total.astype(BF16)
+                send(comb.at[g, i], got.at[g, 1], p_send.at[0], p_recv.at[g], {"sp": where})
+
+    def own_grads(g):
+        with jax.named_scope(f"gotwait{g}"):
+            arrived(got.at[g], p_recv.at[g])
+        total = part[g, me].astype(F32) + got[g, 0].astype(F32) + got[g, 1].astype(F32)
+        keys = k_head[g]
+        inv = lax.rsqrt(head_mean(keys * keys) + norm_eps)
+        back = norm_rotate_back(keys, inv, total, k_gain, cos_own, sin_own)
+        both = jnp.where(low_lanes, back, total).astype(BF16)
+        g_all[g, md] = both
+        mine = g_all.at[g, md]
+        for o in range(2, dp, 2):
+            send(mine, mine, g_send.at[0], gd_recv.at[g], {"dp": dp_peer(o)})
+        send(mine, mine, g_send.at[0], gm_recv.at[g], {"dp": mate})
+        at = slice(g * HEAD_CHANNELS, (g + 1) * HEAD_CHANNELS)
+        own_k[:, at] = both[:, :HEAD_CHANNELS]
+        own_v[:, at] = both[:, HEAD_CHANNELS:]
+
+    def pass_on(g):
+        with jax.named_scope(f"gdwait{g}"):
+            arrived(g_all.at[g, pl.ds(0, near_chips)], gd_recv.at[g])
+        for o in range(2, dp, 2):
+            block = g_all.at[g, dp_from(o)]
+            send(block, block, g_send.at[1], gm_recv.at[g], {"dp": mate})
+
+    def weight_grads(g):
+        with jax.named_scope(f"gmwait{g}"):
+            arrived(g_all.at[g, pl.ds(0, dp // 2)], gm_recv.at[g])
+        total = contract(x_t[...], g_all[g].reshape(dp * rows, LANES), ((1,), (0,)))
+        wg_part[g] = total.astype(BF16).reshape(n, piece, LANES)
         for o in range(1, n):
-            src = sp_from(o)
-            arrived(k_all.at[c, src], kv_recv.at[0, c, src])
-            arrived(v_all.at[c, src], kv_recv.at[1, c, src])
-            stack_keys(c, src)
-        key_low, value_low = attend(2 * c)
-        key_high, value_high = attend(2 * c + 1)
-        both = jnp.concatenate([key_low, key_high, value_low, value_high], axis=1).astype(BF16)
-        for j in range(n):
-            part[c, j] = both[j * rows:(j + 1) * rows, :]
-        for o in order:
-            send(part.at[c, sp_peer(o)], got.at[c, me], p_send.at[c, o], p_recv.at[c, me],
+            send(wg_part.at[g, sp_peer(o)], wg_got.at[g, me], r_send.at[0], r_recv.at[g],
                  {"sp": sp_peer(o)})
 
-    def own_grads(c):
-        total = part[c, me].astype(F32)
+    def sum_weight_grads(g):
+        with jax.named_scope(f"rwait{g}"):
+            arrived(wg_got.at[g, pl.ds(0, last)], r_recv.at[g])
+        total = wg_part[g, me].astype(F32)
         for o in range(1, n):
-            src = sp_from(o)
-            arrived(got.at[c, src], p_recv.at[c, src])
-            total = total + got[c, src].astype(F32)
-        g_all[c, md, :, :LANES] = norm_rotate_back(
-            k_all[c, me].astype(F32), total[:, :LANES], k_gain, cos_own, sin_own
+            total = total + wg_got[g, sp_from(o)].astype(F32)
+        fin_all[g, me] = total.astype(BF16)
+        mine = fin_all.at[g, me]
+        for o in range(1, n):
+            send(mine, mine, r_send.at[1], f_recv.at[g], {"sp": sp_peer(o)})
+
+    def put_weight_grads(g):
+        with jax.named_scope(f"fwait{g}"):
+            arrived(fin_all.at[g, pl.ds(0, last)], f_recv.at[g])
+        total = fin_all[g].reshape(share, LANES).astype(F32)
+        at = slice(g * HEAD_CHANNELS, (g + 1) * HEAD_CHANNELS)
+        kw_buf[:, at] = total[:, :HEAD_CHANNELS]
+        vw_buf[:, at] = total[:, HEAD_CHANNELS:]
+
+    def query_grads(c):
+        dq_buf[:, pair(c)] = norm_rotate_back(
+            q_buf[:, pair(c)].astype(F32), q_inv[:, pair(c)], dq_acc[:, pair(c)],
+            q_gain * score_scale, cos_own, sin_own,
         ).astype(BF16)
-        g_all[c, md, :, LANES:] = total[:, LANES:].astype(BF16)
-        mine = g_all.at[c, md]
-        for o in range(2, dp, 2):
-            send(mine, mine, g_send.at[c, o], g_recv.at[c, md], {"dp": dp_peer(o)})
-        send(mine, mine, g_send.at[c, 1], g_recv.at[c, md], {"dp": mate})
-
-    def pass_on(c):
-        for o in range(2, dp, 2):
-            src = dp_from(o)
-            theirs = g_all.at[c, src]
-            arrived(theirs, g_recv.at[c, src])
-            send(theirs, theirs, g_fsend.at[c, o], g_recv.at[c, src], {"dp": mate})
-
-    def weight_grads(c):
-        total = contract(x_t[md], g_all[c, md], ((1,), (0,)))
-        for o in range(2, dp, 2):
-            src = dp_from(o)
-            total = total + contract(x_t[src], g_all[c, src], ((1,), (0,)))
+
+    def project(src):
+        out = contract(own_k[...], wk_all[src], ((1,), (1,)))
+        out = out + contract(own_v[...], wv_all[src], ((1,), (1,)))
+        dx_buf[:, columns(src)] = out.astype(BF16)
+
+    blocks = q_width // LANES
+    for g in range(heads):
+        with jax.named_scope(f"kvwait{g}"):
+            for role, sources in ((0, (1, 2, 3)), (1, (3,)), (3, (2, 1, 0))):
+                @pl.when(me == role)
+                def _():
+                    for src in sources:
+                        take_kv(src, g)
+        with jax.named_scope(f"attend{g}"):
+            kept = attend(g)
+            send_parts(g)
+            query_part(g, *kept)
+        if g == 0:
+            @pl.when(me == 2)
+            def _():
+                for k in range(2, heads):
+                    relay(3, k, 1)
+        if g == 2:
+            with jax.named_scope("comb0"):
+                combine(0)
+    with jax.named_scope("comb1"):
+        combine(1)
+    with jax.named_scope("xt"):
+        for copy in local[8:]:
+            copy.wait()
+        arrived(x_all.at[pl.ds(0, dp - 1)], x_sem.at[1])
+        for src in range(dp):
+            x_t[:, src * rows:(src + 1) * rows] = x_all[src].T
+    with jax.named_scope("comb2"):
+        combine(2)
+    with jax.named_scope("dqa"):
+        for c in range(blocks // 2):
+            query_grads(c)
+    with jax.named_scope("comb3"):
+        combine(3)
+    for g in range(heads):
+        with jax.named_scope(f"own{g}"):
+            own_grads(g)
+    send_weights(2)
+    with jax.named_scope("dqb"):
+        for c in range(blocks // 2, blocks):
+            query_grads(c)
+    with jax.named_scope("wpass"):
+        pass_weights(0)
+        pass_weights(1)
+    pass_on(0)
+    pass_on(1)
+    for g in range(heads):
+        if g + 2 < heads:
+            pass_on(g + 2)
+        with jax.named_scope(f"wg{g}"):
+            weight_grads(g)
+    with jax.named_scope("sum0"):
+        sum_weight_grads(0)
+    with jax.named_scope("wlate"):
+        pass_weights(2)
+    sum_weight_grads(1)
+    with jax.named_scope("proja"):
         for o in range(0, dp, 2):
-            src = mate_from(o)
-            arrived(g_all.at[c, src], g_recv.at[c, src])
-            total = total + contract(x_t[src], g_all[c, src], ((1,), (0,)))
-        for j in range(n):
-            wg_part[c, j] = total[j * piece:(j + 1) * piece, :].astype(BF16)
-        for o in order:
-            send(wg_part.at[c, sp_peer(o)], wg_got.at[c, me], r_send.at[c, o], r_recv.at[c, me],
-                 {"sp": sp_peer(o)})
-
-    def sum_weight_grads(c):
-        total = wg_part[c, me].astype(F32)
-        for o in range(1, n):
-            src = sp_from(o)
-            arrived(wg_got.at[c, src], r_recv.at[c, src])
-            total = total + wg_got[c, src].astype(F32)
-        fin_all[c, me] = total.astype(BF16)
-        mine = fin_all.at[c, me]
-        for o in order:
-            send(mine, mine, f_send.at[c, o], f_recv.at[c, me], {"sp": sp_peer(o)})
-
-    for o in range(dp):
-        src = dp_from(o)
-        if o:
-            arrived(x_all.at[src], x_recv.at[src])
-        x_t[src] = x_all[src].T
-
-    for c in range(head_pairs):
-        own_grads(c)
-        if c == 0:
-            for kind, (_, dst) in enumerate(weights):
-                for o in range(2, dp, 2):
-                    src = dp_from(o)
-                    arrived(dst.at[src], w_recv.at[kind, src])
-                    send(dst.at[src], dst.at[src], w_fsend.at[kind, o], w_recv.at[kind, src],
-                         {"dp": mate})
-            for i in range(q_width // LANES):
-                dq_buf[:, pair(i)] = norm_rotate_back(
-                    q_buf[:, pair(i)].astype(F32), dq_acc[:, pair(i)], q_gain, cos_own, sin_own
-                ).astype(BF16)
-
-    own = jnp.concatenate(
-        [g_all[c, md, :, :LANES] for c in range(head_pairs)]
-        + [g_all[c, md, :, LANES:] for c in range(head_pairs)], axis=1)
-    kv_width = head_pairs * LANES
-
-    def project(src):
-        out = contract(own[:, :kv_width], wk_all[src], ((1,), (1,)))
-        out = out + contract(own[:, kv_width:], wv_all[src], ((1,), (1,)))
-        dx_buf[:, columns(src)] = out.astype(BF16)
-
-    for c in range(head_pairs):
-        pass_on(c)
-        weight_grads(c)
-    for o in range(0, dp, 2):
-        project(dp_from(o))
-    for o in range(0, dp, 2):
-        src = mate_from(o)
-        for kind, (_, dst) in enumerate(weights):
-            arrived(dst.at[src], w_recv.at[kind, src])
-        project(src)
-    for c in range(head_pairs):
-        sum_weight_grads(c)
-    for c in range(head_pairs):
-        for o in range(n):
-            src = sp_from(o)
-            if o:
-                arrived(fin_all.at[c, src], f_recv.at[c, src])
-            at = pl.ds(pl.multiple_of(src * piece, piece), piece)
-            kw_buf[at, pair(c)] = fin_all[c, src, :, :LANES].astype(F32)
-            vw_buf[at, pair(c)] = fin_all[c, src, :, LANES:].astype(F32)
-    for copy in sends:
-        copy.wait_send()
+            project(dp_from(o))
+    sum_weight_grads(2)
+    sum_weight_grads(3)
+    with jax.named_scope("wfin"):
+        for kind in range(3):
+            finish_weights(kind)
+    with jax.named_scope("projb"):
+        for o in range(0, dp, 2):
+            project(mate_from(o))
+    for g in range(heads):
+        with jax.named_scope(f"put{g}"):
+            put_weight_grads(g)
+
+    with jax.named_scope("drain"):
+        @pl.when(me < last)
+        def _():
+            departed(kv_all.at[me], kv_send.at[0])
+
+        @pl.when(me > 0)
+        def _():
+            departed(kv_all.at[me], kv_send.at[1])
+
+        @pl.when(me == last)
+        def _():
+            departed(kv_all.at[me], kv_send.at[2])
+
+        for role, sources in ((1, (0, 2)), (2, (0, 1, 3))):
+            @pl.when(me == role)
+            def _():
+                for src in sources:
+                    departed(kv_all.at[src], kv_send.at[3 + src])
+
+        departed(x_all.at[pl.ds(0, dp - 1)], x_sem.at[0])
+        for kind, (_, dst, at) in enumerate(weights):
+            departed(dst.at[pl.ds(0, dp - 1), at], w_send.at[kind])
+        departed(part.at[:, pl.ds(0, 3)], p_send.at[0])
+        departed(g_all.at[:, pl.ds(0, dp // 2)], g_send.at[0])
+        departed(g_all.at[:, pl.ds(0, near_chips)], g_send.at[1])
+        departed(wg_part.at[:, pl.ds(0, last)], r_send.at[0])
+        departed(fin_all.at[:, pl.ds(0, last)], r_send.at[1])
 
 
 def write_kernel(*refs):
@@ -563,32 +715,33 @@
     length = rows * n
     share = width // dp
     kv_heads = kv_width // HEAD_CHANNELS
-    half = kv_heads // 2
     stack = rows * (q_width // kv_width)
     cos_tab, sin_tab = pair_tables(length)
     vmem = pltpu.VMEM
     dma = pltpu.SemaphoreType.DMA
-    wide = 2 * LANES
+    packed = (rows, LANES)
     scratch = [
         vmem((1, HEAD_CHANNELS), F32), vmem((1, HEAD_CHANNELS), F32),
         vmem((rows, q_width), BF16), vmem((rows, q_width), BF16),
-        vmem((length, LANES), F32), vmem((length, LANES), F32),
-        vmem((half, n, rows, LANES), BF16), vmem((half, n, rows, LANES), BF16),
-        vmem((dp, rows, share), BF16),
+        vmem(packed, F32), vmem(packed, F32),
+        vmem((rows, kv_width), BF16), vmem((rows, kv_width), BF16),
+        vmem((kv_heads, *packed), F32), vmem((n, kv_heads, *packed), BF16),
+        vmem((rows, q_width), F32),
+        vmem((kv_heads, stack, LANES), BF16), vmem((kv_heads, stack, LANES), BF16),
+        vmem((dp, rows, share), BF16), vmem((share, dp * rows), BF16),
         vmem((dp, share, kv_width), BF16), vmem((dp, share, kv_width), BF16),
-        vmem((kv_heads, stack, HEAD_CHANNELS), BF16), vmem((kv_heads, stack, HEAD_CHANNELS), BF16),
-        vmem((kv_heads, length, HEAD_CHANNELS), BF16), vmem((kv_heads, length, HEAD_CHANNELS), BF16),
         vmem((rows, q_width), F32),
-        vmem((half, n, rows, wide), BF16), vmem((half, n, rows, wide), BF16),
-        vmem((half, dp, rows, wide), BF16), vmem((dp, share, rows), BF16),
-        vmem((half, n, share // n, wide), BF16), vmem((half, n, share // n, wide), BF16),
-        vmem((half, n, share // n, wide), BF16),
-        dma((9 + 2 * half,)),
-        dma((2, half, n)), dma((2, half, n)), dma((dp,)), dma((dp,)),
-        dma((2, dp)), dma((2, dp)), dma((2, dp)),
-        dma((half, n)), dma((half, n)),
-        dma((half, dp)), dma((half, dp)), dma((half, dp)),
-        dma((half, n)), dma((half, n)), dma((half, n)), dma((half, n)),
+        vmem((kv_heads, n, *packed), BF16),
+        vmem((kv_heads, 2, *packed), BF16), vmem((kv_heads, 2, *packed), BF16),
+        vmem((kv_heads, 2, *packed), BF16),
+        vmem((kv_heads, dp, *packed), BF16),
+        vmem((rows, kv_width), BF16), vmem((rows, kv_width), BF16),
+        vmem((kv_heads, n, share // n, LANES), BF16),
+        vmem((kv_heads, n, share // n, LANES), BF16),
+        vmem((kv_heads, n, share // n, LANES), BF16),
+        dma((11,)), dma((3 + n,)), dma((n, kv_heads)), dma((2,)), dma((3,)), dma((3, 2)),
+        dma((1,)), dma((kv_heads, 2)), dma((kv_heads,)),
+        dma((2,)), dma((kv_heads,)), dma((kv_heads,)), dma((2,)), dma((kv_heads,)), dma((kv_heads,)),
     ]
     hbm = pl.BlockSpec(memory_space=pltpu.HBM)
     here = pl.BlockSpec(memory_space=pltpu.VMEM)
@@ -626,8 +779,8 @@
     n = lax.axis_size("sp")
     dp = lax.axis_size("dp")
     rows, width = inputs.shape[1:]
-    fits = dp % 2 == 0 and width % (dp * LANES) == 0 and rows % LANES == 0 and rows * n <= 1024
-    if fits and (width // dp) % (16 * n) == 0:
+    fits = n == 4 and dp == 8 and width % (dp * LANES) == 0 and rows == LANES
+    if fits and (width // dp) % (32 * n) == 0:
         return kernel_step(n, dp, inputs, *rest)
     return on_device(inputs, *rest)
 

time: 49.4 us -> 46.2 us (0.935)
  Pallas kernels: 48.6 us -> 45.4 us
    pallas_call x1, Pallas kernels: 47.5 us -> 44.3 us  [kernel_step(): pl.pallas_call(functools.partial(step_kernel, n, dp), out_shape=[pltpu.VM...]
where the time goes in v1:
time: 46.2 us; the launch traced here: 46 us
  Pallas kernels  45.4 us (98%)
  between operations  0.64 us (1%)
    pallas_call x1, Pallas kernels, kernel_step(): pl.pallas_call(functools.partial(step_kernel, n, dp), out_shape=[pltpu.VM...  44.3 us
    pallas_call x1, Pallas kernels, kernel_step(): pl.pallas_call(write_kernel, out_shape=[jax.ShapeDtypeStruct(shape, kind)...  1.09 us

profile of v1, /device:TPU:0, one launch (start us, length us, event | category | flops | bytes accessed | tf_op | source)
XLA Modules:
  0.0 46.0 jit_solution(4599516003161452347)
XLA Ops:
  0.6 44.3 %shard_map.138 = (bf16[128,2048]{1,0:T(8,128)(2,1)S(1)}, bf16[128,1024]{1,0:T(8,128)(2,1)S(1)}, f32[256,256]{1,0:T(8,128)S(1)}, f32[256,256]{1,0:T(8,128)S(1)}) custom-call(bf16[128,2048]{1,0:T(8,128)(2,1)} %bitcast.9, bf16[128,1024]{1,0:T(8,128)(2,1)} %bitcast.10, bf16[128,256]{1,0:T(8,128)(2,1)} %bitcast.12, bf16[128,256]{1,0:T(8,128)(2,1)} %bitcast.13, ...), custom_call_target="tpu_custom_call" | custom-call | tf_op jit(solution)/shard_map/pallas_call | solution.py:753
  45.0 1.1 %shard_map.139 = (bf16[128,2048]{1,0:T(8,128)(2,1)}, bf16[128,1024]{1,0:T(8,128)(2,1)}, f32[256,256]{1,0:T(8,128)}, f32[256,256]{1,0:T(8,128)}) custom-call(bf16[128,2048]{1,0:T(8,128)(2,1)S(1)} %get-tuple-element.12.refs_0_, bf16[128,1024]{1,0:T(8,128)(2,1)S(1)} %get-tuple-element.13.refs_1_, f32[256,256]{1,0:T(8,128)S(1)} %get-tuple-element.14.refs_2_, ...), custom_call_target="tpu_custom_call" | custom-call | tf_op jit(solution)/shard_map/pallas_call | solution.py:767

commit v2 on v1

--- a/solution.py
+++ b/solution.py
@@ -284,7 +284,7 @@
     dx_buf, dq_buf, kw_buf, vw_buf,
     qg_ref, kg_ref, q_buf, do_buf, cos_buf, sin_buf, k_own, v_own, k_head, kv_all, q_inv, q_st, do_st,
     x_all, x_t, wk_all, wv_all, dq_acc, part, comb_in, comb, got, g_all, own_k, own_v,
-    wg_part, wg_got, fin_all,
+    wg_part, wg_got, fin_all, fin_low,
     local_sem, kv_send, kv_recv, x_sem, w_send, w_recv, p_send, c_recv, p_recv,
     g_send, gd_recv, gm_recv, r_send, r_recv, f_recv,
 ):
@@ -296,14 +296,19 @@
     per_group = q_width // (heads * HEAD_CHANNELS)
     half_share = share // 2
     mate = md + 1 - 2 * (md % 2)
-    piece = share // n
     last = n - 1
+    first_mid = n // 2 - 1
     partner = me + 1 - 2 * (me % 2)
     low_side = me < n // 2
     other_end = jnp.where(low_side, last, 0)
     other_mid = jnp.where(low_side, n // 2, n // 2 - 1)
     is_end = jnp.logical_or(me == 0, me == last)
     near_chips = dp // 2 - 1
+    core = md % 2
+    upper = md + 1 - core
+    side_mid = jnp.where(is_end, partner, me)
+    is_owner = jnp.logical_and(jnp.logical_not(is_end), core == 1)
+    relayed = 1
 
     def sp_peer(o):
         return lax.rem(me + o, n)
@@ -339,9 +344,9 @@
     def _():
         greet({"sp": me + 1})
 
-    @pl.when(me == 0)
+    @pl.when(jnp.logical_not(is_end))
     def _():
-        greet({"sp": last})
+        greet({"sp": other_end})
 
     for o in range(1, dp):
         greet({"dp": dp_peer(o)})
@@ -397,27 +402,15 @@
         k_head[2 * c + 1] = shift(keys)
 
     with jax.named_scope("barrier"):
-        pl.semaphore_wait(
-            barrier, dp - 1 + jnp.where(me > 0, 1, 0) + jnp.where(me < last, 1, 0)
-            + jnp.where(me == last, 1, 0)
-        )
+        pl.semaphore_wait(barrier, dp + 1)
 
     def send_kv(src, g, sem, where):
         block = kv_all.at[src, g]
         send(block, block, kv_send.at[sem], kv_recv.at[src, g], {"sp": where})
 
     for g in range(heads):
-        @pl.when(me < last)
-        def _():
-            send_kv(me, g, 0, me + 1)
-
-        @pl.when(me > 0)
-        def _():
-            send_kv(me, g, 1, me - 1)
-
-        @pl.when(me == last)
-        def _():
-            send_kv(me, g, 2, 0)
+        send_kv(me, g, 0, other_mid)
+        send_kv(me, g, 1, partner)
 
     for o in range(1, dp):
         send(x_hbm.at[:, columns(dp_peer(o))], x_all.at[md], x_sem.at[0], x_sem.at[1],
@@ -469,56 +462,56 @@
 
     def relay(src, g, where):
         take_kv(src, g)
-        send_kv(src, g, 3 + src, where)
-
+        send_kv(src, g, 2 + src, where)
+
+    def relays(turns):
+        @pl.when(jnp.logical_not(is_end))
+        def _():
+            for src, g in turns:
+                relay([other_mid, other_end][src], g, partner)
+
+    turns = sorted(
+        [(0, g) for g in range(heads)] + [(1, g) for g in range(heads)],
+        key=lambda turn: turn[1] + 1.5 * turn[0],
+    )
     with jax.named_scope("relay"):
-        @pl.when(me == 1)
-        def _():
-            for g in range(heads + 2):
-                if g < heads:
-                    relay(0, g, 2)
-                if g >= 2:
-                    relay(2, g - 2, 0)
-
-        @pl.when(me == 2)
-        def _():
-            for g in range(heads):
-                relay(1, g, 3)
-                if g < 2:
-                    relay(3, g, 1)
-                relay(0, g, 3)
+        relays(turns)
 
     def attend(g):
         kv = kv_all[:, g].reshape(n * rows, LANES)
-        queries = q_st[g]
-        grads = do_st[g]
-        scores = contract(kv, queries, ((1,), (1,)))
-        shifted = jnp.exp(scores - jnp.max(scores, axis=0, keepdims=True))
-        prob = shifted * (1.0 / jnp.sum(shifted, axis=0, keepdims=True))
-        prob_grad = contract(kv, grads, ((1,), (1,)))
-        row_dot = jnp.sum(prob * prob_grad, axis=0, keepdims=True)
-        score_grad = (prob * (prob_grad - row_dot)).astype(BF16)
-        both = contract(score_grad, queries, ((1,), (0,)))
-        both = both + contract(prob.astype(BF16), grads, ((1,), (0,)))
+        both = None
+        score_grads = []
+        for r in range(per_group):
+            at = pl.ds(r * rows, rows)
+            queries = q_st[g, at, :]
+            grads = do_st[g, at, :]
+            scores = contract(kv, queries, ((1,), (1,)))
+            prob_grad = contract(kv, grads, ((1,), (1,)))
+            shifted = jnp.exp(scores - jnp.max(scores, axis=0, keepdims=True))
+            prob = shifted * (1.0 / jnp.sum(shifted, axis=0, keepdims=True))
+            row_dot = jnp.sum(prob * prob_grad, axis=0, keepdims=True)
+            score_grad = (prob * (prob_grad - row_dot)).astype(BF16)
+            term = contract(score_grad, queries, ((1,), (0,)))
+            term = term + contract(prob.astype(BF16), grads, ((1,), (0,)))
+            both = term if both is None else both + term
+            score_grads.append(score_grad)
         part[g] = both.astype(BF16).reshape(n, rows, LANES)
-        return kv, score_grad
-
-    def query_part(g, kv, score_grad):
-        dq_t = contract(kv[:, :HEAD_CHANNELS], score_grad, ((0,), (0,)))
+        return kv, score_grads
+
+    def query_part(g, kv, score_grads):
+        parts = [contract(kv[:, :HEAD_CHANNELS], a, ((0,), (0,))) for a in score_grads]
         for r in range(0, per_group, 2):
-            turned = jnp.concatenate(
-                [dq_t[:, r * rows:(r + 1) * rows], dq_t[:, (r + 1) * rows:(r + 2) * rows]], axis=0
-            )
             head = g * per_group + r
-            dq_acc[:, head * HEAD_CHANNELS:head * HEAD_CHANNELS + LANES] = turned.T
+            dq_acc[:, head * HEAD_CHANNELS:head * HEAD_CHANNELS + LANES] = jnp.concatenate(
+                [parts[r], parts[r + 1]], axis=0
+            ).T
 
     def send_parts(g):
         @pl.when(is_end)
         def _():
-            send(part.at[g, other_end], comb_in.at[g, 0], p_send.at[0], c_recv.at[g, 0],
-                 {"sp": partner})
-            send(part.at[g, other_mid], comb_in.at[g, 1], p_send.at[0], c_recv.at[g, 1],
-                 {"sp": partner})
+            for i, where in enumerate([other_end, other_mid]):
+                send(part.at[g, where], comb_in.at[g, i], p_send.at[0], c_recv.at[g, i],
+                     {"sp": partner})
 
         send(part.at[g, partner], got.at[g, 0], p_send.at[0], p_recv.at[g], {"sp": partner})
 
@@ -559,25 +552,57 @@
         with jax.named_scope(f"gmwait{g}"):
             arrived(g_all.at[g, pl.ds(0, dp // 2)], gm_recv.at[g])
         total = contract(x_t[...], g_all[g].reshape(dp * rows, LANES), ((1,), (0,)))
-        wg_part[g] = total.astype(BF16).reshape(n, piece, LANES)
-        for o in range(1, n):
-            send(wg_part.at[g, sp_peer(o)], wg_got.at[g, me], r_send.at[0], r_recv.at[g],
-                 {"sp": sp_peer(o)})
+        wg_part[g] = total.astype(BF16).reshape(2, half_share, LANES)
+
+        def give(half, where):
+            send(wg_part.at[g, half], wg_got.at[g, core * n + me], r_send.at[0],
+                 r_recv.at[g, core], {"sp": where, "dp": upper})
+
+        give(other_mid - first_mid, other_mid)
+
+        @pl.when(jnp.logical_not(is_owner))
+        def _():
+            give(side_mid - first_mid, side_mid)
 
     def sum_weight_grads(g):
-        with jax.named_scope(f"rwait{g}"):
-            arrived(wg_got.at[g, pl.ds(0, last)], r_recv.at[g])
-        total = wg_part[g, me].astype(F32)
-        for o in range(1, n):
-            total = total + wg_got[g, sp_from(o)].astype(F32)
-        fin_all[g, me] = total.astype(BF16)
-        mine = fin_all.at[g, me]
-        for o in range(1, n):
-            send(mine, mine, r_send.at[1], f_recv.at[g], {"sp": sp_peer(o)})
+        @pl.when(is_owner)
+        def _():
+            mine = me - first_mid
+            with jax.named_scope(f"rwait{g}"):
+                arrived(wg_got.at[g, pl.ds(0, last)], r_recv.at[g, 1])
+            total = wg_part[g, mine].astype(F32)
+            for o in range(1, n):
+                total = total + wg_got[g, n + sp_from(o)].astype(F32)
+            fin_all[g, mine] = total.astype(BF16)
+            with jax.named_scope(f"rwaits{g}"):
+                arrived(wg_got.at[g, pl.ds(0, n)], r_recv.at[g, 0])
+            total = wg_got[g, 0].astype(F32)
+            for src in range(1, n):
+                total = total + wg_got[g, src].astype(F32)
+            fin_low[g] = total.astype(BF16)
+            for block, d in ((fin_low.at[g], mate), (fin_all.at[g, mine], md)):
+                for where in (other_mid, partner):
+                    send(block, fin_all.at[g, mine], r_send.at[1], f_recv.at[g],
+                         {"sp": where, "dp": d})
+                if g >= relayed:
+                    send(block, fin_all.at[g, mine], r_send.at[3], f_recv.at[g],
+                         {"sp": other_end, "dp": d})
+            send(fin_low.at[g], fin_all.at[g, mine], r_send.at[1], f_recv.at[g], {"dp": mate})
 
     def put_weight_grads(g):
         with jax.named_scope(f"fwait{g}"):
-            arrived(fin_all.at[g, pl.ds(0, last)], f_recv.at[g])
+            @pl.when(is_owner)
+            def _():
+                arrived(fin_all.at[g, 0], f_recv.at[g])
+
+            @pl.when(jnp.logical_not(is_owner))
+            def _():
+                arrived(fin_all.at[g], f_recv.at[g])
+        if g < relayed:
+            @pl.when(jnp.logical_not(is_end))
+            def _():
+                block = fin_all.at[g, other_mid - first_mid]
+                send(block, block, r_send.at[2], f_recv.at[g], {"sp": partner})
         total = fin_all[g].reshape(share, LANES).astype(F32)
         at = slice(g * HEAD_CHANNELS, (g + 1) * HEAD_CHANNELS)
         kw_buf[:, at] = total[:, :HEAD_CHANNELS]
@@ -597,93 +622,78 @@
     blocks = q_width // LANES
     for g in range(heads):
         with jax.named_scope(f"kvwait{g}"):
-            for role, sources in ((0, (1, 2, 3)), (1, (3,)), (3, (2, 1, 0))):
-                @pl.when(me == role)
-                def _():
-                    for src in sources:
-                        take_kv(src, g)
+            take_kv(partner, g)
+
+            @pl.when(is_end)
+            def _():
+                take_kv(other_mid, g)
+                take_kv(other_end, g)
         with jax.named_scope(f"attend{g}"):
             kept = attend(g)
             send_parts(g)
             query_part(g, *kept)
-        if g == 0:
-            @pl.when(me == 2)
-            def _():
-                for k in range(2, heads):
-                    relay(3, k, 1)
-        if g == 2:
-            with jax.named_scope("comb0"):
-                combine(0)
-    with jax.named_scope("comb1"):
-        combine(1)
     with jax.named_scope("xt"):
         for copy in local[8:]:
             copy.wait()
         arrived(x_all.at[pl.ds(0, dp - 1)], x_sem.at[1])
         for src in range(dp):
             x_t[:, src * rows:(src + 1) * rows] = x_all[src].T
-    with jax.named_scope("comb2"):
-        combine(2)
-    with jax.named_scope("dqa"):
-        for c in range(blocks // 2):
+    def scoped(name, step, *args):
+        with jax.named_scope(name):
+            step(*args)
+
+    def query_half(first):
+        for c in range(first, first + blocks // 2):
             query_grads(c)
-    with jax.named_scope("comb3"):
-        combine(3)
-    for g in range(heads):
-        with jax.named_scope(f"own{g}"):
-            own_grads(g)
+
+    scoped("comb0", combine, 0)
+    scoped("comb1", combine, 1)
+    scoped("dqa", query_half, 0)
+    scoped("own0", own_grads, 0)
+    scoped("comb2", combine, 2)
+    scoped("comb3", combine, 3)
+    scoped("own1", own_grads, 1)
+    scoped("own2", own_grads, 2)
+    scoped("pass0", pass_on, 0)
+    scoped("own3", own_grads, 3)
     send_weights(2)
-    with jax.named_scope("dqb"):
-        for c in range(blocks // 2, blocks):
-            query_grads(c)
+    scoped("dqb", query_half, blocks // 2)
+    scoped("pass1", pass_on, 1)
+    scoped("wg0", weight_grads, 0)
+    scoped("pass2", pass_on, 2)
+    scoped("wg1", weight_grads, 1)
+    scoped("pass3", pass_on, 3)
+    scoped("wg2", weight_grads, 2)
+    scoped("wg3", weight_grads, 3)
     with jax.named_scope("wpass"):
         pass_weights(0)
         pass_weights(1)
-    pass_on(0)
-    pass_on(1)
-    for g in range(heads):
-        if g + 2 < heads:
-            pass_on(g + 2)
-        with jax.named_scope(f"wg{g}"):
-            weight_grads(g)
-    with jax.named_scope("sum0"):
-        sum_weight_grads(0)
-    with jax.named_scope("wlate"):
-        pass_weights(2)
-    sum_weight_grads(1)
+    scoped("sum0", sum_weight_grads, 0)
+    scoped("wlate", pass_weights, 2)
+    scoped("sum1", sum_weight_grads, 1)
     with jax.named_scope("proja"):
         for o in range(0, dp, 2):
             project(dp_from(o))
-    sum_weight_grads(2)
-    sum_weight_grads(3)
+    scoped("sum2", sum_weight_grads, 2)
     with jax.named_scope("wfin"):
         for kind in range(3):
             finish_weights(kind)
     with jax.named_scope("projb"):
         for o in range(0, dp, 2):
             project(mate_from(o))
-    for g in range(heads):
-        with jax.named_scope(f"put{g}"):
-            put_weight_grads(g)
+    scoped("put0", put_weight_grads, 0)
+    scoped("sum3", sum_weight_grads, 3)
+    for g in range(1, heads):
+        scoped(f"put{g}", put_weight_grads, g)
 
     with jax.named_scope("drain"):
-        @pl.when(me < last)
+        departed(kv_all.at[me], kv_send.at[0])
+        departed(kv_all.at[me], kv_send.at[1])
+
+        @pl.when(jnp.logical_not(is_end))
         def _():
-            departed(kv_all.at[me], kv_send.at[0])
-
-        @pl.when(me > 0)
-        def _():
-            departed(kv_all.at[me], kv_send.at[1])
-
-        @pl.when(me == last)
-        def _():
-            departed(kv_all.at[me], kv_send.at[2])
-
-        for role, sources in ((1, (0, 2)), (2, (0, 1, 3))):
-            @pl.when(me == role)
-            def _():
-                for src in sources:
-                    departed(kv_all.at[src], kv_send.at[3 + src])
+            departed(kv_all.at[other_mid], kv_send.at[2 + other_mid])
+            departed(kv_all.at[other_end], kv_send.at[2 + other_end])
 
         departed(x_all.at[pl.ds(0, dp - 1)], x_sem.at[0])
         for kind, (_, dst, at) in enumerate(weights):
@@ -691,8 +701,20 @@
         departed(part.at[:, pl.ds(0, 3)], p_send.at[0])
         departed(g_all.at[:, pl.ds(0, dp // 2)], g_send.at[0])
         departed(g_all.at[:, pl.ds(0, near_chips)], g_send.at[1])
-        departed(wg_part.at[:, pl.ds(0, last)], r_send.at[0])
-        departed(fin_all.at[:, pl.ds(0, last)], r_send.at[1])
+
+        @pl.when(is_owner)
+        def _():
+            departed(wg_part.at[:, 0], r_send.at[0])
+            departed(wg_got.at[:, pl.ds(0, 5)], r_send.at[1])
+            departed(wg_got.at[pl.ds(0, heads - relayed), pl.ds(0, 2)], r_send.at[3])
+
+        @pl.when(jnp.logical_not(is_owner))
+        def _():
+            departed(wg_part, r_send.at[0])
+
+        @pl.when(jnp.logical_not(is_end))
+        def _():
+            departed(fin_low.at[pl.ds(0, relayed)], r_send.at[2])
 
 
 def write_kernel(*refs):
@@ -736,12 +758,13 @@
         vmem((kv_heads, 2, *packed), BF16),
         vmem((kv_heads, dp, *packed), BF16),
         vmem((rows, kv_width), BF16), vmem((rows, kv_width), BF16),
-        vmem((kv_heads, n, share // n, LANES), BF16),
-        vmem((kv_heads, n, share // n, LANES), BF16),
-        vmem((kv_heads, n, share // n, LANES), BF16),
-        dma((11,)), dma((3 + n,)), dma((n, kv_heads)), dma((2,)), dma((3,)), dma((3, 2)),
+        vmem((kv_heads, 2, share // 2, LANES), BF16),
+        vmem((kv_heads, 2 * n, share // 2, LANES), BF16),
+        vmem((kv_heads, 2, share // 2, LANES), BF16), vmem((kv_heads, share // 2, LANES), BF16),
+        dma((11,)), dma((2 + n,)), dma((n, kv_heads)), dma((2,)), dma((3,)), dma((3, 2)),
         dma((1,)), dma((kv_heads, 2)), dma((kv_heads,)),
-        dma((2,)), dma((kv_heads,)), dma((kv_heads,)), dma((2,)), dma((kv_heads,)), dma((kv_heads,)),
+        dma((2,)), dma((kv_heads,)), dma((kv_heads,)),
+        dma((4,)), dma((kv_heads, 2)), dma((kv_heads,)),
     ]
     hbm = pl.BlockSpec(memory_space=pltpu.HBM)
     here = pl.BlockSpec(memory_space=pltpu.VMEM)

time: 46.2 us -> 43.4 us (0.939)
  Pallas kernels: 45.4 us -> 42.5 us
    pallas_call x1, Pallas kernels: 44.3 us -> 41.5 us  [kernel_step(): pl.pallas_call(functools.partial(step_kernel, n, dp), out_shape=[pltpu.VM...]
where the time goes in v2:
time: 43.4 us; the launch traced here: 43.2 us
  Pallas kernels  42.5 us (98%)
  between operations  0.64 us (1%)
    pallas_call x1, Pallas kernels, kernel_step(): pl.pallas_call(functools.partial(step_kernel, n, dp), out_shape=[pltpu.VM...  41.5 us
    pallas_call x1, Pallas kernels, kernel_step(): pl.pallas_call(write_kernel, out_shape=[jax.ShapeDtypeStruct(shape, kind)...  1.09 us

profile of v2, /device:TPU:0, one launch (start us, length us, event | category | flops | bytes accessed | tf_op | source)
XLA Modules:
  0.0 43.2 jit_solution(13882546139736852643)
XLA Ops:
  0.6 41.5 %shard_map.138 = (bf16[128,2048]{1,0:T(8,128)(2,1)S(1)}, bf16[128,1024]{1,0:T(8,128)(2,1)S(1)}, f32[256,256]{1,0:T(8,128)S(1)}, f32[256,256]{1,0:T(8,128)S(1)}) custom-call(bf16[128,2048]{1,0:T(8,128)(2,1)} %bitcast.9, bf16[128,1024]{1,0:T(8,128)(2,1)} %bitcast.10, bf16[128,256]{1,0:T(8,128)(2,1)} %bitcast.12, bf16[128,256]{1,0:T(8,128)(2,1)} %bitcast.13, ...), custom_call_target="tpu_custom_call" | custom-call | tf_op jit(solution)/shard_map/pallas_call | solution.py:776
  42.1 1.1 %shard_map.139 = (bf16[128,2048]{1,0:T(8,128)(2,1)}, bf16[128,1024]{1,0:T(8,128)(2,1)}, f32[256,256]{1,0:T(8,128)}, f32[256,256]{1,0:T(8,128)}) custom-call(bf16[128,2048]{1,0:T(8,128)(2,1)S(1)} %get-tuple-element.12.refs_0_, bf16[128,1024]{1,0:T(8,128)(2,1)S(1)} %get-tuple-element.13.refs_1_, f32[256,256]{1,0:T(8,128)S(1)} %get-tuple-element.14.refs_2_, ...), custom_call_target="tpu_custom_call" | custom-call | tf_op jit(solution)/shard_map/pallas_call | solution.py:790

commit v3 on v2

--- a/solution.py
+++ b/solution.py
@@ -308,6 +308,7 @@
     upper = md + 1 - core
     side_mid = jnp.where(is_end, partner, me)
     is_owner = jnp.logical_and(jnp.logical_not(is_end), core == 1)
+    first_straight = 0
     relayed = 1
 
     def sp_peer(o):
@@ -472,23 +473,26 @@
 
     turns = sorted(
         [(0, g) for g in range(heads)] + [(1, g) for g in range(heads)],
-        key=lambda turn: turn[1] + 1.5 * turn[0],
+        key=lambda turn: turn[1] + 0.5 * turn[0],
     )
     with jax.named_scope("relay"):
         relays(turns)
+
+    step = 1
 
     def attend(g):
         kv = kv_all[:, g].reshape(n * rows, LANES)
         both = None
         score_grads = []
-        for r in range(per_group):
-            at = pl.ds(r * rows, rows)
+        for r in range(0, per_group, step):
+            at = pl.ds(r * rows, step * rows)
             queries = q_st[g, at, :]
             grads = do_st[g, at, :]
             scores = contract(kv, queries, ((1,), (1,)))
             prob_grad = contract(kv, grads, ((1,), (1,)))
             shifted = jnp.exp(scores - jnp.max(scores, axis=0, keepdims=True))
-            prob = shifted * (1.0 / jnp.sum(shifted, axis=0, keepdims=True))
+            inverse = 1.0 / jnp.sum(shifted, axis=0, keepdims=True)
+            prob = shifted * inverse
             row_dot = jnp.sum(prob * prob_grad, axis=0, keepdims=True)
             score_grad = (prob * (prob_grad - row_dot)).astype(BF16)
             term = contract(score_grad, queries, ((1,), (0,)))
@@ -506,8 +510,17 @@
                 [parts[r], parts[r + 1]], axis=0
             ).T
 
+    def straight(g):
+        return core == 0 if g >= first_straight else core < 0
+
     def send_parts(g):
-        @pl.when(is_end)
+        @pl.when(straight(g))
+        def _():
+            for where in (other_end, other_mid):
+                send(part.at[g, where], got.at[g, jnp.where(is_end, 1, 2)], p_send.at[0],
+                     p_recv.at[g], {"sp": where})
+
+        @pl.when(jnp.logical_and(is_end, jnp.logical_not(straight(g))))
         def _():
             for i, where in enumerate([other_end, other_mid]):
                 send(part.at[g, where], comb_in.at[g, i], p_send.at[0], c_recv.at[g, i],
@@ -516,7 +529,7 @@
         send(part.at[g, partner], got.at[g, 0], p_send.at[0], p_recv.at[g], {"sp": partner})
 
     def combine(g):
-        @pl.when(jnp.logical_not(is_end))
+        @pl.when(jnp.logical_not(jnp.logical_or(is_end, straight(g))))
         def _():
             for i, where in enumerate([other_end, other_mid]):
                 arrived(comb_in.at[g, i], c_recv.at[g, i])
@@ -526,8 +539,15 @@
 
     def own_grads(g):
         with jax.named_scope(f"gotwait{g}"):
-            arrived(got.at[g], p_recv.at[g])
+            @pl.when(straight(g))
+            def _():
+                arrived(got.at[g], p_recv.at[g])
+
+            @pl.when(jnp.logical_not(straight(g)))
+            def _():
+                arrived(got.at[g, pl.ds(0, 2)], p_recv.at[g])
         total = part[g, me].astype(F32) + got[g, 0].astype(F32) + got[g, 1].astype(F32)
+        total = total + jnp.where(straight(g), got[g, 2].astype(F32), 0.0)
         keys = k_head[g]
         inv = lax.rsqrt(head_mean(keys * keys) + norm_eps)
         back = norm_rotate_back(keys, inv, total, k_gain, cos_own, sin_own)
@@ -628,6 +648,9 @@
             def _():
                 take_kv(other_mid, g)
                 take_kv(other_end, g)
+        if g == heads - 1:
+            with jax.named_scope("comb0"):
+                combine(0)
         with jax.named_scope(f"attend{g}"):
             kept = attend(g)
             send_parts(g)
@@ -646,44 +669,43 @@
         for c in range(first, first + blocks // 2):
             query_grads(c)
 
-    scoped("comb0", combine, 0)
     scoped("comb1", combine, 1)
     scoped("dqa", query_half, 0)
     scoped("own0", own_grads, 0)
     scoped("comb2", combine, 2)
     scoped("comb3", combine, 3)
     scoped("own1", own_grads, 1)
+    scoped("dqa", query_half, 0)
     scoped("own2", own_grads, 2)
     scoped("pass0", pass_on, 0)
     scoped("own3", own_grads, 3)
     send_weights(2)
     scoped("dqb", query_half, blocks // 2)
-    scoped("pass1", pass_on, 1)
-    scoped("wg0", weight_grads, 0)
-    scoped("pass2", pass_on, 2)
-    scoped("wg1", weight_grads, 1)
-    scoped("pass3", pass_on, 3)
-    scoped("wg2", weight_grads, 2)
-    scoped("wg3", weight_grads, 3)
     with jax.named_scope("wpass"):
         pass_weights(0)
         pass_weights(1)
+    scoped("wg0", weight_grads, 0)
+    scoped("pass1", pass_on, 1)
+    scoped("wg1", weight_grads, 1)
+    scoped("pass2", pass_on, 2)
+    scoped("pass3", pass_on, 3)
     scoped("sum0", sum_weight_grads, 0)
+    scoped("wg2", weight_grads, 2)
+    scoped("wg3", weight_grads, 3)
+    scoped("sum1", sum_weight_grads, 1)
     scoped("wlate", pass_weights, 2)
-    scoped("sum1", sum_weight_grads, 1)
     with jax.named_scope("proja"):
         for o in range(0, dp, 2):
             project(dp_from(o))
     scoped("sum2", sum_weight_grads, 2)
+    scoped("sum3", sum_weight_grads, 3)
     with jax.named_scope("wfin"):
         for kind in range(3):
             finish_weights(kind)
     with jax.named_scope("projb"):
         for o in range(0, dp, 2):
             project(mate_from(o))
-    scoped("put0", put_weight_grads, 0)
-    scoped("sum3", sum_weight_grads, 3)
-    for g in range(1, heads):
+    for g in range(heads):
         scoped(f"put{g}", put_weight_grads, g)
 
     with jax.named_scope("drain"):
@@ -755,7 +777,7 @@
         vmem((rows, q_width), F32),
         vmem((kv_heads, n, *packed), BF16),
         vmem((kv_heads, 2, *packed), BF16), vmem((kv_heads, 2, *packed), BF16),
-        vmem((kv_heads, 2, *packed), BF16),
+        vmem((kv_heads, 3, *packed), BF16),
         vmem((kv_heads, dp, *packed), BF16),
         vmem((rows, kv_width), BF16), vmem((rows, kv_width), BF16),
         vmem((kv_heads, 2, share // 2, LANES), BF16),

time: 43.4 us -> 42.1 us (0.970); the launches traced: 43.2 us -> 41.4 us
  Pallas kernels: 42.5 us -> 40.8 us
    pallas_call x1, Pallas kernels: 41.5 us -> 39.7 us  [kernel_step(): pl.pallas_call(functools.partial(step_kernel, n, dp), out_shape=[pltpu.VM...]
where the time goes in v3:
time: 42.1 us; the launch traced here: 41.4 us
  Pallas kernels  40.8 us (97%)
  between operations  0.64 us (2%)
    pallas_call x1, Pallas kernels, kernel_step(): pl.pallas_call(functools.partial(step_kernel, n, dp), out_shape=[pltpu.VM...  39.7 us
    pallas_call x1, Pallas kernels, kernel_step(): pl.pallas_call(write_kernel, out_shape=[jax.ShapeDtypeStruct(shape, kind)...  1.09 us

profile of v3, /device:TPU:0, one launch (start us, length us, event | category | flops | bytes accessed | tf_op | source)
XLA Modules:
  0.0 41.4 jit_solution(14348177217135333453)
XLA Ops:
  0.6 39.7 %shard_map.138 = (bf16[128,2048]{1,0:T(8,128)(2,1)S(1)}, bf16[128,1024]{1,0:T(8,128)(2,1)S(1)}, f32[256,256]{1,0:T(8,128)S(1)}, f32[256,256]{1,0:T(8,128)S(1)}) custom-call(bf16[128,2048]{1,0:T(8,128)(2,1)} %bitcast.9, bf16[128,1024]{1,0:T(8,128)(2,1)} %bitcast.10, bf16[128,256]{1,0:T(8,128)(2,1)} %bitcast.12, bf16[128,256]{1,0:T(8,128)(2,1)} %bitcast.13, ...), custom_call_target="tpu_custom_call" | custom-call | tf_op jit(solution)/shard_map/pallas_call | solution.py:798
  40.3 1.1 %shard_map.139 = (bf16[128,2048]{1,0:T(8,128)(2,1)}, bf16[128,1024]{1,0:T(8,128)(2,1)}, f32[256,256]{1,0:T(8,128)}, f32[256,256]{1,0:T(8,128)}) custom-call(bf16[128,2048]{1,0:T(8,128)(2,1)S(1)} %get-tuple-element.12.refs_0_, bf16[128,1024]{1,0:T(8,128)(2,1)S(1)} %get-tuple-element.13.refs_1_, f32[256,256]{1,0:T(8,128)S(1)} %get-tuple-element.14.refs_2_, ...), custom_call_target="tpu_custom_call" | custom-call | tf_op jit(solution)/shard_map/pallas_call | solution.py:812

commit v4 on v3

--- a/solution.py
+++ b/solution.py
@@ -282,10 +282,10 @@
     n, dp,
     x_hbm, q_hbm, k_hbm, v_hbm, do_hbm, qg_hbm, kg_hbm, km_hbm, vm_hbm, cos_hbm, sin_hbm,
     dx_buf, dq_buf, kw_buf, vw_buf,
-    qg_ref, kg_ref, q_buf, do_buf, cos_buf, sin_buf, k_own, v_own, k_head, kv_all, q_inv, q_st, do_st,
+    qg_ref, kg_ref, q_buf, do_buf, cos_buf, sin_buf, k_own, v_own, k_head, k_inv, kv_all, q_inv, q_st, do_st,
     x_all, x_t, wk_all, wv_all, dq_acc, part, comb_in, comb, got, g_all, own_k, own_v,
     wg_part, wg_got, fin_all, fin_low,
-    local_sem, kv_send, kv_recv, x_sem, w_send, w_recv, p_send, c_recv, p_recv,
+    ready, local_sem, kv_send, kv_recv, x_sem, w_send, w_recv, p_send, c_recv, p_recv,
     g_send, gd_recv, gm_recv, r_send, r_recv, f_recv,
 ):
     me = lax.axis_index("sp")
@@ -349,8 +349,16 @@
     def _():
         greet({"sp": other_end})
 
-    for o in range(1, dp):
-        greet({"dp": dp_peer(o)})
+    def flip(bit):
+        return md + bit - 2 * bit * ((md // bit) % 2)
+
+    x_side, y_side = flip(2), flip(4)
+    corner = x_side + y_side - md
+    beside = [mate]
+    for d in (x_side, y_side):
+        beside += [d, d + mate - md]
+    for d in beside:
+        greet({"dp": d})
 
     my_rows = pl.ds(pl.multiple_of(me * rows, rows), rows)
     wanted = [
@@ -396,14 +404,16 @@
     for c in range(heads // 2):
         keys = k_own[:, pair(c)].astype(F32)
         vals = v_own[:, pair(c)].astype(F32)
-        turned = norm_rotate(keys, k_gain, cos_own, sin_own)[0]
+        turned, inv = norm_rotate(keys, k_gain, cos_own, sin_own)
         kv_all[me, 2 * c] = jnp.where(low_lanes, turned, shift(vals)).astype(BF16)
         kv_all[me, 2 * c + 1] = jnp.where(low_lanes, shift(turned), vals).astype(BF16)
         k_head[2 * c] = keys
         k_head[2 * c + 1] = shift(keys)
+        k_inv[2 * c] = inv
+        k_inv[2 * c + 1] = shift(inv)
 
     with jax.named_scope("barrier"):
-        pl.semaphore_wait(barrier, dp + 1)
+        pl.semaphore_wait(barrier, 2 + len(beside))
 
     def send_kv(src, g, sem, where):
         block = kv_all.at[src, g]
@@ -413,21 +423,24 @@
         send_kv(me, g, 0, other_mid)
         send_kv(me, g, 1, partner)
 
-    for o in range(1, dp):
-        send(x_hbm.at[:, columns(dp_peer(o))], x_all.at[md], x_sem.at[0], x_sem.at[1],
-             {"dp": dp_peer(o)})
+    pl.semaphore_signal(ready, inc=1, device_id={"dp": x_side}, device_id_type=MESH)
+
+    def send_tokens(peers):
+        for d in peers:
+            send(x_hbm.at[:, columns(d)], x_all.at[md], x_sem.at[0], x_sem.at[1], {"dp": d})
+
+    send_tokens(beside)
 
     top = pl.ds(0, half_share)
     bottom = pl.ds(half_share, half_share)
     full = pl.ds(0, share)
     weights = [(km_hbm, wk_all, full), (vm_hbm, wv_all, top), (vm_hbm, wv_all, bottom)]
 
-    def send_weights(kind):
+    def send_weights(kind, peers):
         src, dst, at = weights[kind]
-        for o in range(2, dp, 2):
-            send(src.at[at], dst.at[md, at], w_send.at[kind], w_recv.at[kind, 0],
-                 {"dp": dp_peer(o)})
-        send(src.at[at], dst.at[md, at], w_send.at[kind], w_recv.at[kind, 1], {"dp": mate})
+        for d in peers:
+            send(src.at[at], dst.at[md, at], w_send.at[kind],
+                 w_recv.at[kind, 1 if d is mate else 0], {"dp": d})
 
     def pass_weights(kind):
         _, dst, at = weights[kind]
@@ -440,8 +453,8 @@
         _, dst, at = weights[kind]
         arrived(dst.at[pl.ds(0, dp // 2), at], w_recv.at[kind, 1])
 
-    send_weights(0)
-    send_weights(1)
+    for kind in range(2):
+        send_weights(kind, (x_side, y_side, mate))
 
     with jax.named_scope("local2"):
         for copy in local[6:8]:
@@ -457,6 +470,11 @@
                 to = pl.ds((r + a) * rows, rows)
                 q_st[g, to, :] = jnp.where(low_lanes, query, 0.0).astype(BF16)
                 do_st[g, to, :] = jnp.where(low_lanes, 0.0, grad).astype(BF16)
+
+    pl.semaphore_wait(ready, 1)
+    send_tokens((corner, corner + mate - md))
+    for kind in range(2):
+        send_weights(kind, (corner,))
 
     def take_kv(src, g):
         arrived(kv_all.at[src, g], kv_recv.at[src, g])
@@ -549,8 +567,7 @@
         total = part[g, me].astype(F32) + got[g, 0].astype(F32) + got[g, 1].astype(F32)
         total = total + jnp.where(straight(g), got[g, 2].astype(F32), 0.0)
         keys = k_head[g]
-        inv = lax.rsqrt(head_mean(keys * keys) + norm_eps)
-        back = norm_rotate_back(keys, inv, total, k_gain, cos_own, sin_own)
+        back = norm_rotate_back(keys, k_inv[g], total, k_gain, cos_own, sin_own)
         both = jnp.where(low_lanes, back, total).astype(BF16)
         g_all[g, md] = both
         mine = g_all.at[g, md]
@@ -601,28 +618,38 @@
                 total = total + wg_got[g, src].astype(F32)
             fin_low[g] = total.astype(BF16)
             for block, d in ((fin_low.at[g], mate), (fin_all.at[g, mine], md)):
-                for where in (other_mid, partner):
-                    send(block, fin_all.at[g, mine], r_send.at[1], f_recv.at[g],
-                         {"sp": where, "dp": d})
                 if g >= relayed:
                     send(block, fin_all.at[g, mine], r_send.at[3], f_recv.at[g],
                          {"sp": other_end, "dp": d})
+                for where in (partner, other_mid):
+                    send(block, fin_all.at[g, mine], r_send.at[1], f_recv.at[g],
+                         {"sp": where, "dp": d})
             send(fin_low.at[g], fin_all.at[g, mine], r_send.at[1], f_recv.at[g], {"dp": mate})
+
+    def hand_on(g):
+        block = fin_all.at[g, other_mid - first_mid]
+        send(block, block, r_send.at[2], f_recv.at[g], {"sp": partner})
+
+    def relay_weight_grads(g):
+        @pl.when(is_owner)
+        def _():
+            arrived(fin_all.at[g, 0], f_recv.at[g])
+            hand_on(g)
 
     def put_weight_grads(g):
         with jax.named_scope(f"fwait{g}"):
-            @pl.when(is_owner)
-            def _():
-                arrived(fin_all.at[g, 0], f_recv.at[g])
+            if g >= relayed:
+                @pl.when(is_owner)
+                def _():
+                    arrived(fin_all.at[g, 0], f_recv.at[g])
 
             @pl.when(jnp.logical_not(is_owner))
             def _():
                 arrived(fin_all.at[g], f_recv.at[g])
         if g < relayed:
-            @pl.when(jnp.logical_not(is_end))
+            @pl.when(jnp.logical_not(jnp.logical_or(is_end, is_owner)))
             def _():
-                block = fin_all.at[g, other_mid - first_mid]
-                send(block, block, r_send.at[2], f_recv.at[g], {"sp": partner})
+                hand_on(g)
         total = fin_all[g].reshape(share, LANES).astype(F32)
         at = slice(g * HEAD_CHANNELS, (g + 1) * HEAD_CHANNELS)
         kw_buf[:, at] = total[:, :HEAD_CHANNELS]
@@ -655,31 +682,30 @@
             kept = attend(g)
             send_parts(g)
             query_part(g, *kept)
+    def scoped(name, step, *args):
+        with jax.named_scope(name):
+            step(*args)
+
+    def query_half(first):
+        for c in range(first, first + blocks // 2):
+            query_grads(c)
+
+    scoped("comb1", combine, 1)
+    scoped("comb2", combine, 2)
+    scoped("comb3", combine, 3)
+    scoped("dqa", query_half, 0)
+    scoped("own0", own_grads, 0)
+    scoped("own1", own_grads, 1)
     with jax.named_scope("xt"):
         for copy in local[8:]:
             copy.wait()
         arrived(x_all.at[pl.ds(0, dp - 1)], x_sem.at[1])
         for src in range(dp):
             x_t[:, src * rows:(src + 1) * rows] = x_all[src].T
-    def scoped(name, step, *args):
-        with jax.named_scope(name):
-            step(*args)
-
-    def query_half(first):
-        for c in range(first, first + blocks // 2):
-            query_grads(c)
-
-    scoped("comb1", combine, 1)
-    scoped("dqa", query_half, 0)
-    scoped("own0", own_grads, 0)
-    scoped("comb2", combine, 2)
-    scoped("comb3", combine, 3)
-    scoped("own1", own_grads, 1)
-    scoped("dqa", query_half, 0)
     scoped("own2", own_grads, 2)
     scoped("pass0", pass_on, 0)
     scoped("own3", own_grads, 3)
-    send_weights(2)
+    send_weights(2, (x_side, y_side, corner, mate))
     scoped("dqb", query_half, blocks // 2)
     with jax.named_scope("wpass"):
         pass_weights(0)
@@ -697,6 +723,7 @@
     with jax.named_scope("proja"):
         for o in range(0, dp, 2):
             project(dp_from(o))
+    scoped("hand0", relay_weight_grads, 0)
     scoped("sum2", sum_weight_grads, 2)
     scoped("sum3", sum_weight_grads, 3)
     with jax.named_scope("wfin"):
@@ -769,7 +796,8 @@
         vmem((rows, q_width), BF16), vmem((rows, q_width), BF16),
         vmem(packed, F32), vmem(packed, F32),
         vmem((rows, kv_width), BF16), vmem((rows, kv_width), BF16),
-        vmem((kv_heads, *packed), F32), vmem((n, kv_heads, *packed), BF16),
+        vmem((kv_heads, *packed), F32), vmem((kv_heads, *packed), F32),
+        vmem((n, kv_heads, *packed), BF16),
         vmem((rows, q_width), F32),
         vmem((kv_heads, stack, LANES), BF16), vmem((kv_heads, stack, LANES), BF16),
         vmem((dp, rows, share), BF16), vmem((share, dp * rows), BF16),
@@ -783,7 +811,7 @@
         vmem((kv_heads, 2, share // 2, LANES), BF16),
         vmem((kv_heads, 2 * n, share // 2, LANES), BF16),
         vmem((kv_heads, 2, share // 2, LANES), BF16), vmem((kv_heads, share // 2, LANES), BF16),
-        dma((11,)), dma((2 + n,)), dma((n, kv_heads)), dma((2,)), dma((3,)), dma((3, 2)),
+        pltpu.SemaphoreType.REGULAR, dma((11,)), dma((2 + n,)), dma((n, kv_heads)), dma((2,)), dma((3,)), dma((3, 2)),
         dma((1,)), dma((kv_heads, 2)), dma((kv_heads,)),
         dma((2,)), dma((kv_heads,)), dma((kv_heads,)),
         dma((4,)), dma((kv_heads, 2)), dma((kv_heads,)),

time: 42.1 us -> 40.7 us (0.967); the launches traced: 41.4 us -> 40.5 us
  Pallas kernels: 40.8 us -> 39.8 us
    pallas_call x1, Pallas kernels: 39.7 us -> 38.8 us  [kernel_step(): pl.pallas_call(functools.partial(step_kernel, n, dp), out_shape=[pltpu.VM...]
where the time goes in v4:
time: 40.7 us; the launch traced here: 40.5 us
  Pallas kernels  39.8 us (98%)
  between operations  0.64 us (2%)
    pallas_call x1, Pallas kernels, kernel_step(): pl.pallas_call(functools.partial(step_kernel, n, dp), out_shape=[pltpu.VM...  38.8 us
    pallas_call x1, Pallas kernels, kernel_step(): pl.pallas_call(write_kernel, out_shape=[jax.ShapeDtypeStruct(shape, kind)...  1.09 us

profile of v4, /device:TPU:0, one launch (start us, length us, event | category | flops | bytes accessed | tf_op | source)
XLA Modules:
  0.0 40.5 jit_solution(9077384330134853241)
XLA Ops:
  0.6 38.8 %shard_map.138 = (bf16[128,2048]{1,0:T(8,128)(2,1)S(1)}, bf16[128,1024]{1,0:T(8,128)(2,1)S(1)}, f32[256,256]{1,0:T(8,128)S(1)}, f32[256,256]{1,0:T(8,128)S(1)}) custom-call(bf16[128,2048]{1,0:T(8,128)(2,1)} %bitcast.9, bf16[128,1024]{1,0:T(8,128)(2,1)} %bitcast.10, bf16[128,256]{1,0:T(8,128)(2,1)} %bitcast.12, bf16[128,256]{1,0:T(8,128)(2,1)} %bitcast.13, ...), custom_call_target="tpu_custom_call" | custom-call | tf_op jit(solution)/shard_map/pallas_call | solution.py:826
  39.4 1.1 %shard_map.139 = (bf16[128,2048]{1,0:T(8,128)(2,1)}, bf16[128,1024]{1,0:T(8,128)(2,1)}, f32[256,256]{1,0:T(8,128)}, f32[256,256]{1,0:T(8,128)}) custom-call(bf16[128,2048]{1,0:T(8,128)(2,1)S(1)} %get-tuple-element.12.refs_0_, bf16[128,1024]{1,0:T(8,128)(2,1)S(1)} %get-tuple-element.13.refs_1_, f32[256,256]{1,0:T(8,128)S(1)} %get-tuple-element.14.refs_2_, ...), custom_call_target="tpu_custom_call" | custom-call | tf_op jit(solution)/shard_map/pallas_call | solution.py:840

commit v5 on v4

--- a/solution.py
+++ b/solution.py
@@ -571,8 +571,8 @@
         both = jnp.where(low_lanes, back, total).astype(BF16)
         g_all[g, md] = both
         mine = g_all.at[g, md]
-        for o in range(2, dp, 2):
-            send(mine, mine, g_send.at[0], gd_recv.at[g], {"dp": dp_peer(o)})
+        for d in (corner, x_side, y_side):
+            send(mine, mine, g_send.at[0], gd_recv.at[g], {"dp": d})
         send(mine, mine, g_send.at[0], gm_recv.at[g], {"dp": mate})
         at = slice(g * HEAD_CHANNELS, (g + 1) * HEAD_CHANNELS)
         own_k[:, at] = both[:, :HEAD_CHANNELS]
@@ -605,25 +605,29 @@
         @pl.when(is_owner)
         def _():
             mine = me - first_mid
+            with jax.named_scope(f"rwaits{g}"):
+                arrived(wg_got.at[g, pl.ds(0, n)], r_recv.at[g, 0])
+            total = wg_got[g, 0].astype(F32)
+            for src in range(1, n):
+                total = total + wg_got[g, src].astype(F32)
+            fin_low[g] = total.astype(BF16)
+
+            def give_out(block, d):
+                if g >= relayed:
+                    send(block, fin_all.at[g, mine], r_send.at[3], f_recv.at[g],
+                         {"sp": other_end, "dp": d})
+                for where in (partner, other_mid):
+                    send(block, fin_all.at[g, mine], r_send.at[1], f_recv.at[g],
+                         {"sp": where, "dp": d})
+
+            give_out(fin_low.at[g], mate)
             with jax.named_scope(f"rwait{g}"):
                 arrived(wg_got.at[g, pl.ds(0, last)], r_recv.at[g, 1])
             total = wg_part[g, mine].astype(F32)
             for o in range(1, n):
                 total = total + wg_got[g, n + sp_from(o)].astype(F32)
             fin_all[g, mine] = total.astype(BF16)
-            with jax.named_scope(f"rwaits{g}"):
-                arrived(wg_got.at[g, pl.ds(0, n)], r_recv.at[g, 0])
-            total = wg_got[g, 0].astype(F32)
-            for src in range(1, n):
-                total = total + wg_got[g, src].astype(F32)
-            fin_low[g] = total.astype(BF16)
-            for block, d in ((fin_low.at[g], mate), (fin_all.at[g, mine], md)):
-                if g >= relayed:
-                    send(block, fin_all.at[g, mine], r_send.at[3], f_recv.at[g],
-                         {"sp": other_end, "dp": d})
-                for where in (partner, other_mid):
-                    send(block, fin_all.at[g, mine], r_send.at[1], f_recv.at[g],
-                         {"sp": where, "dp": d})
+            give_out(fin_all.at[g, mine], md)
             send(fin_low.at[g], fin_all.at[g, mine], r_send.at[1], f_recv.at[g], {"dp": mate})
 
     def hand_on(g):

time: 40.7 us -> 40.7 us (level)
  no operation moved by 1% of the time
where the time goes in v5:
time: 40.7 us; the launch traced here: 40.5 us
  Pallas kernels  39.8 us (98%)
  between operations  0.64 us (2%)
    pallas_call x1, Pallas kernels, kernel_step(): pl.pallas_call(functools.partial(step_kernel, n, dp), out_shape=[pltpu.VM...  38.8 us
    pallas_call x1, Pallas kernels, kernel_step(): pl.pallas_call(write_kernel, out_shape=[jax.ShapeDtypeStruct(shape, kind)...  1.09 us

profile of v5, /device:TPU:0, one launch (start us, length us, event | category | flops | bytes accessed | tf_op | source)
XLA Modules:
  0.0 40.5 jit_solution(4667414237646354959)
XLA Ops:
  0.6 38.8 %shard_map.138 = (bf16[128,2048]{1,0:T(8,128)(2,1)S(1)}, bf16[128,1024]{1,0:T(8,128)(2,1)S(1)}, f32[256,256]{1,0:T(8,128)S(1)}, f32[256,256]{1,0:T(8,128)S(1)}) custom-call(bf16[128,2048]{1,0:T(8,128)(2,1)} %bitcast.9, bf16[128,1024]{1,0:T(8,128)(2,1)} %bitcast.10, bf16[128,256]{1,0:T(8,128)(2,1)} %bitcast.12, bf16[128,256]{1,0:T(8,128)(2,1)} %bitcast.13, ...), custom_call_target="tpu_custom_call" | custom-call | tf_op jit(solution)/shard_map/pallas_call | solution.py:830
  39.4 1.1 %shard_map.139 = (bf16[128,2048]{1,0:T(8,128)(2,1)}, bf16[128,1024]{1,0:T(8,128)(2,1)}, f32[256,256]{1,0:T(8,128)}, f32[256,256]{1,0:T(8,128)}) custom-call(bf16[128,2048]{1,0:T(8,128)(2,1)S(1)} %get-tuple-element.12.refs_0_, bf16[128,1024]{1,0:T(8,128)(2,1)S(1)} %get-tuple-element.13.refs_1_, f32[256,256]{1,0:T(8,128)S(1)} %get-tuple-element.14.refs_2_, ...), custom_call_target="tpu_custom_call" | custom-call | tf_op jit(solution)/shard_map/pallas_call | solution.py:844
